TPU v7x, 128 devices: a whole 4x4x4 slice. The times are simulated.
128 devices in a mesh: sp: 16 (over z, y), fs: 4 (over x), tp: 2 (over core).
Axes of the slice: x: 4, y: 4, z: 4, core: 2. Of those that a mesh axis runs over, the one named last changes fastest.
Arguments:
- tokens: bfloat16 [4, 4096, 2048], P('fs', 'sp', 'tp'), may hold values from -6 to 6
- norm_gain: float32 [2048], replicated, may hold values from 0.1 to 1.9
- lin_query: bfloat16 [2048, 1024], P(None, ('fs', 'tp')), may hold values from -0.125 to 0.125
- lin_key: bfloat16 [2048, 1024], P(None, ('fs', 'tp')), may hold values from -0.125 to 0.125
- lin_value: bfloat16 [2048, 2048], P(None, ('fs', 'tp')), may hold values from -0.125 to 0.125
- lin_decay: bfloat16 [2048, 1024], P(None, ('fs', 'tp')), may hold values from -0.125 to 0.125
- decay_bias: float32 [1024], replicated, may hold values from -0.5 to 8.5
- decay_shift: bfloat16 [2, 4, 4096], P(None, 'fs', 'sp'), may hold values from -1.4 to 1.5, as said below
- soft_query: bfloat16 [2048, 2048], P(None, ('fs', 'tp')), may hold values from -0.190034947 to 0.190034947
- soft_key: bfloat16 [2048, 2048], P(None, ('fs', 'tp')), may hold values from -1.9887378 to 1.9887378
- soft_value: bfloat16 [2048, 2048], P(None, ('fs', 'tp')), may hold values from -0.125 to 0.125
- soft_lambda: float32 [8], replicated, may hold values from 0.3 to 0.8
- lin_gain: float32 [256], replicated, may hold values from 0.1 to 1.9
- soft_gain: float32 [256], replicated, may hold values from 0.1 to 1.9
- lin_out: bfloat16 [2048, 2048], P(('fs', 'tp')), may hold values from -0.09375 to 0.09375
- soft_out: bfloat16 [2048, 2048], P(('fs', 'tp')), may hold values from -0.09375 to 0.09375
Outputs:
- mixed: bfloat16 [4, 4096, 2048], P('fs', 'sp', 'tp')
- log_mass: float32 [8, 2, 4, 4096], P(('fs', 'tp'), None, None, 'sp')
Inputs may be any that keep to these rules, and one draw needn't show every extreme that they name: `decay_shift`: row 1 is never positive.
All inputs are finite; a program needn't handle non-finite values.
Results may differ from a plain program's by a relative error of at most 0.02.
Values may be sent and summed in bfloat16 or wider, within the bound.
No kernel may reach another device: no remote copies, remote signals or barrier semaphores. Data moves between devices by JAX's collectives and lax.ppermute only.
A program may use at most 192 MiB of HBM per device.

v0:
```python
from functools import partial

import jax
import jax.numpy as jnp
from jax import lax
from jax.experimental import pallas as pl
from jax.experimental.pallas import tpu as pltpu
from jax.sharding import Mesh
from jax.sharding import PartitionSpec as P


KEY = 128
VALUE = 256
SP = ("sp_0", "sp_1")
GRID = ("sp_0", "sp_1", "tp")
ROW = ("fs", "tp")
ROWS = 256
EXTRA = 16

norm_eps = 1e-06
decay_tau = 16.0
rope_base = 500000.0
LOG2E = 1.4426950408889634
LN2 = 0.6931471805599453

NT = (((1,), (1,)), ((), ()))
TN = (((0,), (0,)), ((), ()))
bf16 = jnp.bfloat16
f32 = jnp.float32


def dot(a, b, dims=(((1,), (0,)), ((), ()))):
    return lax.dot_general(a, b, dims, preferred_element_type=f32)


def ring(length, shift):
    return [(i, (i + shift) % length) for i in range(length)]


def axis_perm(shift, first):
    pairs = []
    for z in range(4):
        for y in range(4):
            for c in range(2):
                along_z = (c == 0) == first
                tz, ty = ((z + shift) % 4, y) if along_z else (z, (y + shift) % 4)
                pairs.append(((z * 4 + y) * 2 + c, (tz * 4 + ty) * 2 + c))
    return pairs


def query_perm(k, back=False):
    pairs = []
    for p in range(4):
        for o in range(4):
            for c in range(2):
                tp, to = (p + k) % 4, o if p in (0, 3) else 3 - o
                here, there = ((p, o), (tp, to)) if c == 0 else ((o, p), (to, tp))
                pairs.append(tuple((i * 4 + j) * 2 + c for i, j in ((there, here) if back else (here, there))))
    return pairs


def core_ring(shift):
    return [(x * 2 + c, ((x + (shift if c == 0 else 4 - shift)) % 4) * 2 + c) for x in range(4) for c in range(2)]


def shift_fs(array, shift):
    return lax.ppermute(array, "fs", ring(4, shift))


def swap(array):
    return lax.ppermute(array, "tp", ring(2, 1))


def scalars():
    return pl.BlockSpec(memory_space=pltpu.SMEM)


def whole():
    return pl.BlockSpec(memory_space=pltpu.VMEM)


def params(mib):
    return pltpu.CompilerParams(vmem_limit_bytes=mib * 1024 * 1024)


def front_kernel(core_ref, mine, other, gain, w_sk, w_sv, w_sq, cos_t, sin_t, kv_out, q_out, normed_out):
    x0 = mine[...].astype(f32)
    x1 = other[...].astype(f32)
    total = jnp.sum(x0 * x0, axis=1, keepdims=True) + jnp.sum(x1 * x1, axis=1, keepdims=True)
    inv = lax.rsqrt(total * (1.0 / 2048.0) + norm_eps)
    half = x0.shape[1]
    here = pl.multiple_of(core_ref[0] * half, half)
    there = pl.multiple_of((1 - core_ref[0]) * half, half)
    normed_out[:, pl.ds(here, half)] = (x0 * inv * gain[:, pl.ds(here, half)]).astype(bf16)
    normed_out[:, pl.ds(there, half)] = (x1 * inv * gain[:, pl.ds(there, half)]).astype(bf16)
    normed = normed_out[...]
    cos_v = cos_t[...]
    sin_v = sin_t[...]

    def rotate(values):
        return values * cos_v + pltpu.roll(values, 64, 1) * sin_v

    sk = dot(normed, w_sk[...])
    for m in range(2):
        kv_out[:, m * KEY : (m + 1) * KEY] = rotate(sk[:, m * KEY : (m + 1) * KEY]).astype(bf16)
    kv_out[:, 2 * KEY :] = dot(normed, w_sv[...]).T.astype(bf16)
    sq = dot(normed, w_sq[...])
    scale = (KEY ** (-0.5)) * LOG2E
    for m in range(2):
        q_out[m * KEY : (m + 1) * KEY, :] = (rotate(sq[:, m * KEY : (m + 1) * KEY]) * scale).T.astype(bf16)


def front(*operands):
    return pl.pallas_call(
        front_kernel,
        in_specs=[scalars()] + [whole()] * (len(operands) - 1),
        out_shape=tuple(jax.ShapeDtypeStruct((ROWS, cols), bf16) for cols in (4 * KEY, 2 * KEY, 2048)),
        name="front",
        compiler_params=params(14),
        cost_estimate=pl.CostEstimate(flops=1500000000, transcendentals=0, bytes_accessed=6000000),
    )(*operands)


def gla_kernel(
    n0, n1, n2, n3, shifts, w_lv, w_d, w_lq, w_lk, bias, local_out, carried_out, state_out, normed_ref, w_lqk
):
    for n, source in enumerate((n0, n1, n2, n3)):
        normed_ref[n] = source[...]
    w_lqk[:, :KEY] = w_lq[...]
    w_lqk[:, KEY:] = w_lk[...]

    def one(n, carry):
        gla_chunk(
            normed_ref[n], shifts[n], w_lv, w_d, w_lqk, bias, local_out.at[n], carried_out.at[n], state_out.at[n]
        )
        return carry

    lax.fori_loop(0, 4, one, 0)


def gla_chunk(normed, shift, w_lv, w_d, w_lqk, bias, local_out, carried_out, state_out):
    pick = lax.broadcasted_iota(jnp.int32, (EXTRA, KEY), 0)
    pick0 = jnp.where(pick == 0, 1.0, 0.0).astype(bf16)
    pick1 = jnp.where(pick == 1, 1.0, 0.0).astype(bf16)
    gate = dot(normed, w_d[...]) + bias[...] + dot(shift, pick0, TN)
    log_sig = jnp.minimum(gate, 0.0) - jnp.log1p(jnp.exp(-jnp.abs(gate)))
    log_decay = log_sig * (1.0 / decay_tau) + dot(shift, pick1, TN)
    v = dot(normed, w_lv[...]).astype(bf16)
    lqk = dot(normed, w_lqk[...])
    q = lqk[:, :KEY].astype(bf16).astype(f32)
    k = lqk[:, KEY:].astype(bf16).astype(f32)

    row = lax.broadcasted_iota(jnp.int32, (ROWS, KEY), 0)
    irow = lax.broadcasted_iota(jnp.int32, (KEY, KEY), 0)
    icol = lax.broadcasted_iota(jnp.int32, (KEY, KEY), 1)
    diff = irow ^ icol
    itself = jnp.sum(q * k, axis=1, keepdims=True)
    halves = [jnp.where(diff == 0, itself[n * KEY : (n + 1) * KEY], 0.0) for n in range(2)]
    inside = log_decay
    group = log_decay
    step = 1
    while step < ROWS:
        second = (row & step) != 0
        decay = jnp.exp(jnp.where(second, inside, group - inside))
        scaled = (jnp.where(second, q, k) * decay).astype(bf16)
        if 2 * step == ROWS:
            cross = dot(scaled[KEY:], scaled[:KEY], NT)
        else:
            keep = (diff < 2 * step) & ((irow & step) != 0) & ((icol & step) == 0)
            for n in range(2):
                part = scaled[n * KEY : (n + 1) * KEY]
                halves[n] = halves[n] + jnp.where(keep, dot(part, part, NT), 0.0)
        before = pltpu.roll(group, step, 0)
        after = pltpu.roll(group, ROWS - step, 0)
        inside = inside + jnp.where(second, before, 0.0)
        group = group + jnp.where(second, before, after)
        step *= 2
    local_out[:KEY] = dot(halves[0].astype(bf16), v[:KEY])
    local_out[KEY:] = dot(jnp.concatenate([cross, halves[1]], axis=1).astype(bf16), v)
    carried_out[...] = (q * jnp.exp(inside)).astype(bf16)
    kept = (k * jnp.exp(group - inside)).astype(bf16)
    state_out[:VALUE, :] = dot(v, kept, TN).astype(bf16)
    state_out[VALUE:, :] = jnp.exp(group[:EXTRA, :]).astype(bf16)


def gla(normed, shifts, weights, bias):
    return pl.pallas_call(
        gla_kernel,
        in_specs=[whole()] * 10,
        out_shape=(
            jax.ShapeDtypeStruct((4, ROWS, VALUE), f32),
            jax.ShapeDtypeStruct((4, ROWS, KEY), bf16),
            jax.ShapeDtypeStruct((4, VALUE + EXTRA, KEY), bf16),
        ),
        scratch_shapes=[pltpu.VMEM((4, ROWS, 2048), bf16), pltpu.VMEM((2048, 2 * KEY), bf16)],
        name="gla",
        compiler_params=params(16),
        cost_estimate=pl.CostEstimate(flops=6000000000, transcendentals=0, bytes_accessed=9000000),
    )(*normed, shifts, *weights, bias)


def ordered(place, parts, j):
    k = (place - j) & 3
    value = parts[0]
    for n in range(1, 4):
        value = jnp.where(k == n, parts[n], value)
    return value


def prefix_kernel(place_ref, g0, g1, g2, g3, before_out, total_out):
    place = place_ref[0]
    parts = [g[...].astype(f32) for g in (g0, g1, g2, g3)]
    state = jnp.zeros((VALUE, KEY), f32)
    keep = jnp.ones((1, KEY), f32)
    for j in range(4):
        before_out[j, :VALUE, :] = state
        before_out[j, VALUE:, :] = jnp.broadcast_to(keep, (EXTRA, KEY))
        part = ordered(place, parts, j)
        own = part[VALUE : VALUE + 1, :]
        state = own * state + part[:VALUE, :]
        keep = own * keep
    total_out[:VALUE, :] = state.astype(bf16)
    total_out[VALUE:, :] = jnp.broadcast_to(keep, (EXTRA, KEY)).astype(bf16)


def prefix(place, parts):
    shape = (VALUE + EXTRA, KEY)
    return pl.pallas_call(
        prefix_kernel,
        in_specs=[scalars()] + [whole()] * 4,
        out_shape=(jax.ShapeDtypeStruct((4,) + shape, f32), jax.ShapeDtypeStruct(shape, bf16)),
        name="prefix",
        compiler_params=params(8),
    )(place, *parts)


def combine_kernel(place_ref, t0, t1, t2, t3, before, o0, o1, o2, o3):
    parts = [t[...].astype(f32) for t in (t0, t1, t2, t3)]
    state = jnp.zeros((VALUE, KEY), f32)
    chosen = state
    for j in range(4):
        chosen = jnp.where(place_ref[0] == j, state, chosen)
        part = ordered(place_ref[0], parts, j)
        state = part[VALUE : VALUE + 1, :] * state + part[:VALUE, :]
    for k, out in enumerate((o0, o1, o2, o3)):
        j = (place_ref[1] + k) & 3
        out[...] = (before[j, VALUE : VALUE + 1, :] * chosen + before[j, :VALUE, :]).astype(bf16)


def combine(places, totals, before):
    return pl.pallas_call(
        combine_kernel,
        in_specs=[scalars()] + [whole()] * 5,
        out_shape=tuple(jax.ShapeDtypeStruct((VALUE, KEY), bf16) for _ in range(4)),
        name="combine",
        compiler_params=params(8),
    )(places, *totals, before)


def lin_kernel(index_ref, i0, i1, i2, i3, local, carried, gain, out):
    for n in range(4):
        which = index_ref[n]
        state_in = i0[...]
        for m, later in enumerate((i1, i2, i3)):
            state_in = jnp.where(which == m + 1, later[...], state_in)
        raw = local[n] + dot(carried[n], state_in, NT)
        mean = jnp.mean(raw * raw, axis=1, keepdims=True)
        out[n] = (raw * lax.rsqrt(mean + norm_eps) * gain[...]).astype(bf16)


def lin_final(index, states, local, carried, gain):
    return pl.pallas_call(
        lin_kernel,
        in_specs=[scalars()] + [whole()] * 7,
        out_shape=jax.ShapeDtypeStruct((4, ROWS, VALUE), bf16),
        name="lin_final",
        compiler_params=params(12),
    )(index, *states, local, carried, gain)


def attend_kernel(near, ids_ref, slot_ids_ref, lam_ref, *refs):
    count_parts = 6 if near else 2
    q_refs, refs = refs[:4], refs[4:]
    parts, refs = refs[:count_parts], refs[count_parts:]
    if near:
        acc, top, total, items, q_all, kv, s_even, s_odd, p_even, p_odd, keep_even, keep_odd, sems = refs
    else:
        acc_in, top, total, gain, out0, out1, out2, out3, items, q_all, kv, s_even, s_odd, p_even, p_odd = refs[:15]
        keep_even, keep_odd, sems, acc, top_in, total_in, mass_ref, mix = refs[15:]
        top_in[...] = top[...]
        total_in[...] = total[...]
        top, total = top_in, total_in
        acc[...] = acc_in[...]
    copies = [
        pltpu.make_async_copy(source, kv.at[pl.ds(2 * n, 2)], sems.at[n]) for n, source in enumerate(parts)
    ]
    for copy in copies:
        copy.start()
    if near:
        acc[...] = jnp.zeros(acc.shape, f32)
        top[...] = jnp.full(top.shape, -jnp.inf, f32)
        total[...] = jnp.zeros(total.shape, f32)
    for n, source in enumerate(q_refs):
        q_all[n] = source[...]
    p_odd[...] = jnp.zeros(p_odd.shape, bf16)
    keep_odd[...] = jnp.ones(keep_odd.shape, f32)

    def collect(n, count):
        items[count] = n
        return count + jnp.where(slot_ids_ref[n >> 2] <= ids_ref[n & 3], 1, 0)

    count = lax.fori_loop(0, 8 * count_parts, collect, 0)
    visible = lax.broadcasted_iota(jnp.int32, (ROWS, ROWS), 0) <= lax.broadcasted_iota(jnp.int32, (ROWS, ROWS), 1)

    def item(i):
        n = items[i]
        return n >> 2, n & 3

    def arrive(slot, before):
        @pl.when((slot >> 1) != (before >> 1))
        def _():
            def wait(n, carry):
                pltpu.make_async_copy(parts[0], kv.at[pl.ds(2 * n, 2)], sems.at[n]).wait()
                return carry

            lax.fori_loop((before >> 1) + 1, (slot >> 1) + 1, wait, 0)

    def scores(after, slot, g, m):
        after[m] = dot(kv[slot, :, m * KEY : (m + 1) * KEY], q_all[g, m * KEY : (m + 1) * KEY, :])

    def mask(after, slot, g):
        @pl.when(slot_ids_ref[slot] == ids_ref[g])
        def _():
            for m in range(2):
                after[m] = jnp.where(visible, after[m], -jnp.inf)

    def weigh(now, p_now, keep_now, g, m):
        old = top[g, m][:1]
        peak = jnp.maximum(old, jnp.max(now[m], axis=0, keepdims=True))
        keep = jnp.exp2(old - peak)
        p = jnp.exp2(now[m] - peak)
        top[g, m] = jnp.broadcast_to(peak, (8, ROWS))
        total[g, m] = total[g, m] * keep + jnp.sum(p, axis=0, keepdims=True)
        keep_now[m] = jnp.broadcast_to(keep, (8, ROWS))
        p_now[m] = p.astype(bf16)

    def add(p_then, keep_then, slot, g, m):
        acc[g, m] = acc[g, m] * keep_then[m][:1] + dot(kv[slot, :, 2 * KEY :], p_then[m])

    def stage(i, now, after, p_now, p_then, keep_now, keep_then):
        slot_then, g_then = item(jnp.maximum(i - 1, 0))
        slot_now, g_now = item(i)
        slot_next, g_next = item(jnp.minimum(i + 1, count - 1))
        arrive(slot_next, slot_now)
        for m in range(2):
            scores(after, slot_next, g_next, m)
            weigh(now, p_now, keep_now, g_now, m)
            add(p_then, keep_then, slot_then, g_then, m)
        mask(after, slot_next, g_next)

    def run():
        first_slot, first_g = item(0)
        arrive(first_slot, -1)
        for m in range(2):
            scores(s_even, first_slot, first_g, m)
        mask(s_even, first_slot, first_g)

        def pair(n, carry):
            stage(2 * n, s_even, s_odd, p_even, p_odd, keep_even, keep_odd)

            @pl.when(2 * n + 1 < count)
            def _():
                stage(2 * n + 1, s_odd, s_even, p_odd, p_even, keep_odd, keep_even)

            return carry

        lax.fori_loop(0, (count + 1) >> 1, pair, 0)
        last_slot, last_g = item(count - 1)
        arrive(2 * count_parts - 1, last_slot)

        @pl.when((count & 1) == 1)
        def _():
            for m in range(2):
                add(p_even, keep_even, last_slot, last_g, m)

        @pl.when((count & 1) == 0)
        def _():
            for m in range(2):
                add(p_odd, keep_odd, last_slot, last_g, m)

    if near:
        pl.when(count > 0)(run)
        pl.when(count == 0)(lambda: arrive(2 * count_parts - 1, -1))
        return
    pl.when(count > 0)(run)
    pl.when(count == 0)(lambda: arrive(2 * count_parts - 1, -1))

    def finish(g, carry):
        sums = [total[g, m][:1] for m in range(2)]
        raw = acc[g, 0] * (1.0 / sums[0]) - acc[g, 1] * (lam_ref[0] / sums[1])
        mean = jnp.mean(raw * raw, axis=0, keepdims=True)
        mix[g, :ROWS] = ((raw * lax.rsqrt(mean + norm_eps)).T * gain[...]).astype(bf16)
        for m in range(2):
            left = jnp.broadcast_to(LN2 * top[g, m][:1] + jnp.log(sums[m]), (8, ROWS))
            lines = jnp.zeros((8, ROWS), f32)
            row = lax.broadcasted_iota(jnp.int32, (8, ROWS), 0)
            for n in range(3):
                part = left.astype(bf16).astype(f32)
                lines = jnp.where(row == n, part, lines)
                left = left - part
            mass_ref[m * 8 : (m + 1) * 8] = lines
        mix[g, ROWS:] = mass_ref[...].astype(bf16)
        return carry

    lax.fori_loop(0, 4, finish, 0)
    for n, out in enumerate((out0, out1, out2, out3)):
        out[...] = mix[n]


SUMS = ((4, 2, VALUE, ROWS), (4, 2, 8, ROWS), (4, 2, 8, ROWS))


def attend(near, ids, slot_ids, lam, queries, parts, *rest):
    scratch = [
        pltpu.SMEM((72,), jnp.int32),
        pltpu.VMEM((4, 2 * KEY, ROWS), bf16),
        pltpu.VMEM((2 * len(parts), ROWS, 4 * KEY), bf16),
        pltpu.VMEM((2, ROWS, ROWS), f32),
        pltpu.VMEM((2, ROWS, ROWS), f32),
        pltpu.VMEM((2, ROWS, ROWS), bf16),
        pltpu.VMEM((2, ROWS, ROWS), bf16),
        pltpu.VMEM((2, 8, ROWS), f32),
        pltpu.VMEM((2, 8, ROWS), f32),
        pltpu.SemaphoreType.DMA((len(parts),)),
    ]
    if near:
        out_shape = tuple(jax.ShapeDtypeStruct(shape, f32) for shape in SUMS)
    else:
        out_shape = tuple(jax.ShapeDtypeStruct((ROWS + EXTRA, VALUE), bf16) for _ in range(4))
        scratch += [pltpu.VMEM(shape, f32) for shape in SUMS]
        scratch += [pltpu.VMEM((EXTRA, ROWS), f32), pltpu.VMEM((4, ROWS + EXTRA, VALUE), bf16)]
    anywhere = pl.BlockSpec(memory_space=pl.ANY)
    return pl.pallas_call(
        partial(attend_kernel, near),
        in_specs=[scalars()] * 3 + [whole()] * 4 + [anywhere] * len(parts) + [whole()] * len(rest),
        out_shape=out_shape,
        scratch_shapes=scratch,
        name="attend_near" if near else "attend_far",
        compiler_params=params(18),
        cost_estimate=pl.CostEstimate(flops=4000000000, transcendentals=0, bytes_accessed=4000000),
    )(ids, slot_ids, lam, *queries, *parts, *rest)


def mixed_rows(index_ref, at, lin, lin_other, soft, soft_other):
    a = index_ref[at]
    b = index_ref[4 + at]
    e = index_ref[8 + at]
    return jnp.concatenate([lin[a], lin_other[a], soft[b, :ROWS], soft_other[e, :ROWS]], axis=1)


def send_kernel(index_ref, lin, lin_other, soft, soft_other, weight, far_out):
    far_out[...] = dot(mixed_rows(index_ref, 0, lin, lin_other, soft, soft_other), weight[...]).astype(bf16)


def keep_kernel(index_ref, lin, lin_other, soft, soft_other, weight, near_out, last_out, own_out):
    near_out[...] = dot(mixed_rows(index_ref, 1, lin, lin_other, soft, soft_other), weight[...]).astype(bf16)
    last_out[...] = dot(mixed_rows(index_ref, 2, lin, lin_other, soft, soft_other), weight[...])
    own_out[...] = dot(mixed_rows(index_ref, 3, lin, lin_other, soft, soft_other), weight[...])


def out_call(kernel, kinds, index, *operands):
    return pl.pallas_call(
        kernel,
        in_specs=[scalars()] + [whole()] * len(operands),
        out_shape=tuple(jax.ShapeDtypeStruct((ROWS, 1024), kind) for kind in kinds),
        compiler_params=params(14),
    )(index, *operands)


def shards(
    tokens, norm_gain, lin_query, lin_key, lin_value, lin_decay, decay_bias, decay_shift,
    soft_query, soft_key, soft_value, soft_lambda, lin_gain, soft_gain, lin_out, soft_out,
):
    x = lax.axis_index("fs")
    c = lax.axis_index("tp")
    z = lax.axis_index("sp_0")
    y = lax.axis_index("sp_1")
    head = x * 2 + c
    own = tokens[0]

    from_low = shift_fs(own, 1)
    from_high = shift_fs(own, 3)
    shifts = [jnp.pad(decay_shift.reshape(2, ROWS), ((0, EXTRA - 2), (0, 0)))]
    shifts += [shift_fs(shifts[0], 4 - d) for d in (1, 2, 3)]

    positions = (z * 4 + y) * ROWS + jnp.arange(ROWS, dtype=jnp.int32)
    inv_freq = jnp.power(f32(rope_base), -jnp.arange(64, dtype=f32) * (2.0 / KEY))
    angles = positions.astype(f32)[:, None] * inv_freq[None, :]
    cos = jnp.cos(angles)
    sin = jnp.sin(angles)
    cos_t = jnp.concatenate([cos, cos], axis=1)
    sin_t = jnp.concatenate([-sin, sin], axis=1)
    bias = lax.dynamic_slice_in_dim(decay_bias, head * KEY, KEY, 0).reshape(1, KEY)
    lam = lax.dynamic_slice_in_dim(soft_lambda, head, 1, 0)
    gain = norm_gain.reshape(1, -1)
    core = c.reshape(1)

    def run_front(chunk):
        other = swap(chunk)
        return front(core, chunk, other, gain, soft_key, soft_value, soft_query, cos_t, sin_t)

    def columns(matrix):
        half = matrix.shape[1] // 2
        mine = lax.dynamic_slice_in_dim(matrix, c * half, half, 1)
        return [mine, swap(lax.dynamic_slice_in_dim(matrix, (1 - c) * half, half, 1))]

    out_weight = jnp.concatenate(columns(lin_out) + columns(soft_out), axis=0)

    fronts = {0: run_front(own)}
    passed = jnp.where(c == 0, from_low, from_high)
    from_far = lax.ppermute(passed, ROW, core_ring(1))
    fronts[1] = run_front(from_high)
    fronts[3] = run_front(from_low)
    fronts[2] = run_front(from_far)
    kv, queries, normed = zip(*(fronts[d] for d in range(4)))
    kv, queries = jnp.stack(kv), jnp.stack(queries)
    local, carried, states = gla(normed, jnp.stack(shifts), (lin_value, lin_decay, lin_query, lin_key), bias)

    r = jnp.where(c == 0, z, y)
    q = jnp.where(c == 0, y, z)

    def piece(stacked, place, k):
        return lax.dynamic_index_in_dim(stacked, (place + k - x) & 3, 0, keepdims=False)

    own_kv = [piece(kv, r, 0)]
    for k in (1, 3, 2):
        own_kv.append(lax.ppermute(piece(kv, r, k), GRID, axis_perm(k, True)))
    own_kv = [own_kv[n] for n in (0, 1, 3, 2)]
    my_q = [lax.ppermute(piece(queries, r, k), GRID, query_perm(k)) for k in range(4)]
    y_parts = [piece(states, y, 0)]
    y_parts += [lax.ppermute(piece(states, y, k), "sp_1", ring(4, k)) for k in (1, 2, 3)]

    own_a = jnp.stack(own_kv[:2])
    own_b = jnp.stack(own_kv[2:])
    low_a = lax.ppermute(own_a, GRID, axis_perm(1, False))
    high_a = lax.ppermute(own_a, GRID, axis_perm(3, False))
    low_b = lax.ppermute(own_b, GRID, axis_perm(1, False))
    high_b = lax.ppermute(own_b, GRID, axis_perm(3, False))
    far_a = lax.ppermute(low_a, GRID, axis_perm(1, False))
    far_b = lax.ppermute(high_b, GRID, axis_perm(3, False))

    before, total = prefix(y.reshape(1), y_parts)
    z_parts = [total] + [lax.ppermute(total, "sp_0", ring(4, k)) for k in (1, 2, 3)]
    coming = combine(jnp.stack([z, y]), z_parts, before)
    coming = [coming[0]] + [lax.ppermute(coming[k], "sp_1", ring(4, k)) for k in (1, 2, 3)]
    k4 = jnp.arange(4, dtype=jnp.int32)
    lin_mix = lin_final((y - x - k4) & 3, coming, local, carried, lin_gain.reshape(1, -1))
    lin_other = swap(lin_mix)

    p = (r - k4) & 3
    source = jnp.where((p == 0) | (p == 3), q, 3 - q)
    ids = jnp.where(c == 0, 4 * p + source, 4 * source + p)
    k16 = jnp.arange(16, dtype=jnp.int32)
    away = jnp.where(k16 < 4, 0, jnp.where(k16 < 8, 1, jnp.where(k16 < 12, 3, 2)))
    block_p = (r - k16) & 3
    block_q = (q - away) & 3
    slot_ids = jnp.where(c == 0, 4 * block_p + block_q, 4 * block_q + block_p)
    sums = attend(
        True, ids, slot_ids[:12], lam, my_q, (own_a, own_b, low_a, low_b, high_a, high_b)
    )
    mix = attend(False, ids, slot_ids[12:], lam, my_q, (far_a, far_b), *sums, soft_gain.reshape(1, -1))

    soft_mix = jnp.stack([lax.ppermute(mix[k], GRID, query_perm(k, True)) for k in range(4)])
    lines = soft_mix[:, ROWS:].reshape(4, 2, 8, ROWS).astype(f32)
    mass_rows = lines[:, :, 0] + lines[:, :, 1] + lines[:, :, 2]
    log_mass = mass_rows[(k4 - r) & 3].transpose(1, 0, 2)[None]

    soft_other = swap(soft_mix)
    pieces = jnp.stack([jnp.int32(2), 3 - 2 * c, 1 + 2 * c, jnp.int32(0)])
    index = jnp.concatenate([pieces, (pieces + x - r) & 3, (pieces + x - q) & 3])
    rows = (lin_mix, lin_other, soft_mix, soft_other, out_weight)
    (far,) = out_call(send_kernel, (bf16,), index, *rows)
    passed = lax.ppermute(far, ROW, core_ring(1))
    near, last, mixed = out_call(keep_kernel, (bf16, f32, f32), index, *rows)
    near_in = lax.ppermute(near, ROW, core_ring(3))
    far_in = lax.ppermute((last + passed.astype(f32)).astype(bf16), ROW, core_ring(1))
    mixed = mixed + near_in.astype(f32) + far_in.astype(f32)
    return (mixed.astype(bf16)[None], log_mass)


def solution(mesh):
    split = Mesh(
        mesh.devices.reshape(4, 4, mesh.shape["fs"], mesh.shape["tp"]), ("sp_0", "sp_1", "fs", "tp")
    )
    heads = P(None, ("fs", "tp"))
    placed = (
        P("fs", SP, "tp"), P(), heads, heads, heads, heads, P(), P(None, "fs", SP),
        heads, heads, heads, P(), P(), P(), P(("fs", "tp"), None), P(("fs", "tp"), None),
    )

    return jax.shard_map(
        shards,
        mesh=split,
        in_specs=placed,
        out_specs=(P("fs", SP, "tp"), P(("fs", "tp"), None, None, SP)),
        check_vma=False,
    )
```

profile of v0, /device:TPU:0, one launch (start us, length us, event | category | flops | bytes accessed | tf_op | source)
XLA Modules:
  0.0 174.7 jit_solution(11310637586907574928)
XLA Ops:
  7.7 8.0 %collective-permute-done.3.mine = bf16[256,1024]{1,0:T(8,128)(2,1)S(1)} collective-permute-done((bf16[256,1024]{1,0:T(8,128)(2,1)}, bf16[256,1024]{1,0:T(8,128)(2,1)S(1)}, u32[]{:S(2)}, u32[]{:S(2)}) %collective-permute-start.3) | collective-permute-done | bytes 524320 | tf_op jit(solution)/shard_map/ppermute | solution.py:67
  21.1 6.6 %collective-permute-done.4.mine = bf16[256,1024]{1,0:T(8,128)(2,1)} collective-permute-done((bf16[256,1024]{1,0:T(8,128)(2,1)}, bf16[256,1024]{1,0:T(8,128)(2,1)}, u32[]{:S(2)}, u32[]{:S(2)}) %collective-permute-start.4) | collective-permute-done | bytes 524320 | tf_op jit(solution)/shard_map/ppermute | solution.py:521
  33.1 2.9 %front.7 = (bf16[256,512]{1,0:T(8,128)(2,1)S(1)}, bf16[256,256]{1,0:T(8,128)(2,1)S(1)}, bf16[256,2048]{1,0:T(8,128)(2,1)S(1)}) custom-call(s32[1]{0:T(128)} %bitcast.4.core_ref, bf16[256,1024]{1,0:T(8,128)(2,1)S(1)} %collective-permute-done.3.mine, bf16[256,1024]{1,0:T(8,128)(2,1)} %collective-permute-done.6.other, f32[1,2048]{1,0:T(1,128)S(1)} %bitcast.84, ...), custom_call_target="tpu_custom_call" | custom-call | flops 1500000000 | bytes 6000000 | tf_op jit(solution)/shard_map/front/pallas_call | solution.py:114
  36.0 2.9 %front.5 = (bf16[256,512]{1,0:T(8,128)(2,1)S(1)}, bf16[256,256]{1,0:T(8,128)(2,1)S(1)}, bf16[256,2048]{1,0:T(8,128)(2,1)S(1)}) custom-call(s32[1]{0:T(128)} %bitcast.4.core_ref, bf16[256,1024]{1,0:T(8,128)(2,1)S(1)} %collective-permute-done.1.mine, bf16[256,1024]{1,0:T(8,128)(2,1)} %collective-permute-done.2.other, f32[1,2048]{1,0:T(1,128)S(1)} %bitcast.85, ...), custom_call_target="tpu_custom_call" | custom-call | flops 1500000000 | bytes 6000000 | tf_op jit(solution)/shard_map/front/pallas_call | solution.py:114
  38.9 2.9 %front.6 = (bf16[256,512]{1,0:T(8,128)(2,1)S(1)}, bf16[256,256]{1,0:T(8,128)(2,1)S(1)}, bf16[256,2048]{1,0:T(8,128)(2,1)S(1)}) custom-call(s32[1]{0:T(128)} %bitcast.4.core_ref, bf16[256,1024]{1,0:T(8,128)(2,1)} %collective-permute-done.4.mine, bf16[256,1024]{1,0:T(8,128)(2,1)S(1)} %collective-permute-done.5.other, f32[1,2048]{1,0:T(1,128)S(1)} %bitcast.86, ...), custom_call_target="tpu_custom_call" | custom-call | flops 1500000000 | bytes 6000000 | tf_op jit(solution)/shard_map/front/pallas_call | solution.py:114
  42.1 4.0 %collective-permute-start.27 = (bf16[256,512]{1,0:T(8,128)(2,1)S(1)}, bf16[256,512]{1,0:T(8,128)(2,1)S(1)}, u32[]{:S(2)}, u32[]{:S(2)}) collective-permute-start(bf16[256,512]{1,0:T(8,128)(2,1)S(1)} %get-tuple-element.72), channel_id=1, source_target_pairs={{0,64},{1,17},{8,72},{9,25},{16,80},{17,1},{24,88},{25,9},{32,96},... | collective-permute-start | bytes 786440 | tf_op jit(solution)/shard_map/ppermute | solution.py:537
  48.0 7.1 %gla.1 = (f32[4,256,256]{2,1,0:T(8,128)S(1)}, bf16[4,256,128]{2,1,0:T(8,128)(2,1)S(1)}, bf16[4,272,128]{2,1,0:T(8,128)(2,1)S(1)}) custom-call(bf16[256,2048]{1,0:T(8,128)(2,1)S(1)} %get-tuple-element.33.n0, bf16[256,2048]{1,0:T(8,128)(2,1)S(1)} %get-tuple-element.34.n1, bf16[256,2048]{1,0:T(8,128)(2,1)S(1)} %get-tuple-element.35.n2, ...), custom_call_target="tpu_custom_call" | custom-call | flops 6000000000 | bytes 9000000 | tf_op jit(solution)/shard_map/gla/pallas_call | solution.py:187
  55.2 3.1 %collective-permute-start.12 = (bf16[272,128]{1,0:T(8,128)(2,1)S(1)}, bf16[272,128]{1,0:T(8,128)(2,1)S(1)}, u32[]{:S(2)}, u32[]{:S(2)}) collective-permute-start(bf16[272,128]{1,0:T(8,128)(2,1)S(1)} %get-tuple-element.80), channel_id=1, source_target_pairs={{0,24},{8,0},{16,8},{24,16},{1,25},{9,1},{17,9},{25,17},{2,26},{10... | collective-permute-start | bytes 208904 | tf_op jit(solution)/shard_map/ppermute | solution.py:541
  58.5 3.3 %collective-permute-start.29 = (bf16[2,256,512]{2,1,0:T(8,128)(2,1)S(1)}, bf16[2,256,512]{2,1,0:T(8,128)(2,1)}, u32[]{:S(2)}, u32[]{:S(2)}) collective-permute-start(bf16[2,256,512]{2,1,0:T(8,128)(2,1)S(1)} %pad_maximum_fusion.5.refs_5_), channel_id=1, source_target_pairs={{0,24},{1,97},{8,0},{9,105},{16,8},{17,113},{24,16},{25,121},{32,5... | collective-permute-start | bytes 1572872 | tf_op jit(solution)/shard_map/ppermute | solution.py:548
  65.4 5.0 %collective-permute-done.11.g2 = bf16[272,128]{1,0:T(8,128)(2,1)S(1)} collective-permute-done((bf16[272,128]{1,0:T(8,128)(2,1)S(1)}, bf16[272,128]{1,0:T(8,128)(2,1)S(1)}, u32[]{:S(2)}, u32[]{:S(2)}) %collective-permute-start.11) | collective-permute-done | bytes 69664 | tf_op jit(solution)/shard_map/ppermute | solution.py:541
  70.4 3.0 %collective-permute-start.32 = (bf16[2,256,512]{2,1,0:T(8,128)(2,1)S(1)}, bf16[2,256,512]{2,1,0:T(8,128)(2,1)}, u32[]{:S(2)}, u32[]{:S(2)}) collective-permute-start(bf16[2,256,512]{2,1,0:T(8,128)(2,1)S(1)} %pad_maximum_fusion.4.refs_4_), channel_id=1, source_target_pairs={{0,24},{1,97},{8,0},{9,105},{16,8},{17,113},{24,16},{25,121},{32,5... | collective-permute-start | bytes 1572872 | tf_op jit(solution)/shard_map/ppermute | solution.py:546
  74.6 12.7 %collective-permute-done.22.refs_2_ = bf16[256,256]{1,0:T(8,128)(2,1)S(1)} collective-permute-done((bf16[256,256]{1,0:T(8,128)(2,1)S(1)}, bf16[256,256]{1,0:T(8,128)(2,1)S(1)}, u32[]{:S(2)}, u32[]{:S(2)}) %collective-permute-start.22) | collective-permute-done | bytes 131104 | tf_op jit(solution)/shard_map/ppermute | solution.py:539
  87.4 3.2 %collective-permute-start.30 = (bf16[2,256,512]{2,1,0:T(8,128)(2,1)}, bf16[2,256,512]{2,1,0:T(8,128)(2,1)}, u32[]{:S(2)}, u32[]{:S(2)}) collective-permute-start(bf16[2,256,512]{2,1,0:T(8,128)(2,1)} %collective-permute-done.29.refs_9_), channel_id=1, source_target_pairs={{0,24},{1,97},{8,0},{9,105},{16,8},{17,113},{24,16},{25,121},{32,5... | collective-permute-start | bytes 1572872 | tf_op jit(solution)/shard_map/ppermute | solution.py:550
  97.4 3.7 %collective-permute-start.15 = (bf16[272,128]{1,0:T(8,128)(2,1)S(1)}, bf16[272,128]{1,0:T(8,128)(2,1)S(1)}, u32[]{:S(2)}, u32[]{:S(2)}) collective-permute-start(bf16[272,128]{1,0:T(8,128)(2,1)S(1)} %get-tuple-element.38.t0), channel_id=1, source_target_pairs={{0,96},{32,0},{64,32},{96,64},{1,97},{33,1},{65,33},{97,65},{2,98}... | collective-permute-start | bytes 208904 | tf_op jit(solution)/shard_map/ppermute | solution.py:553
  101.1 2.9 %collective-permute-start.14 = (bf16[272,128]{1,0:T(8,128)(2,1)S(1)}, bf16[272,128]{1,0:T(8,128)(2,1)S(1)}, u32[]{:S(2)}, u32[]{:S(2)}) collective-permute-start(bf16[272,128]{1,0:T(8,128)(2,1)S(1)} %get-tuple-element.38.t0), channel_id=1, source_target_pairs={{0,64},{32,96},{64,0},{96,32},{1,65},{33,97},{65,1},{97,33},{2,66}... | collective-permute-start | bytes 208904 | tf_op jit(solution)/shard_map/ppermute | solution.py:553
  104.9 10.5 %attend_near.1 = (f32[4,2,256,256]{3,2,1,0:T(8,128)S(1)}, f32[4,2,8,256]{3,2,1,0:T(8,128)S(1)}, f32[4,2,8,256]{3,2,1,0:T(8,128)S(1)}) custom-call(s32[4]{0:T(128)S(1)} %broadcast_select_fusion.2.ids_ref, s32[12]{0:T(128)S(1)} %bitcast.78, f32[1]{0:T(128)} %dynamic_slice.62.lam_ref, bf16[256,256]{1,0:T(8,128)(2,1)S(1)} %collective-permute-done.20.refs_0_, ...), custom_call_target="tpu_custom_call" | custom-call | flops 4000000000 | bytes 4000000 | tf_op jit(solution)/shard_map/attend_near/pallas_call | solution.py:443
  115.4 6.1 %attend_far.1 = (bf16[272,256]{1,0:T(8,128)(2,1)S(1)}, bf16[272,256]{1,0:T(8,128)(2,1)S(1)}, bf16[272,256]{1,0:T(8,128)(2,1)S(1)}, bf16[272,256]{1,0:T(8,128)(2,1)S(1)}) custom-call(s32[4]{0:T(128)S(1)} %broadcast_select_fusion.2.ids_ref, s32[4]{0:T(128)S(1)} %slice.18.slot_ids_ref, f32[1]{0:T(128)} %dynamic_slice.62.lam_ref, ...), custom_call_target="tpu_custom_call" | custom-call | flops 4000000000 | bytes 4000000 | tf_op jit(solution)/shard_map/attend_far/pallas_call | solution.py:443
  122.8 8.5 %collective-permute-start.35 = (bf16[272,256]{1,0:T(8,128)(2,1)S(1)}, bf16[272,256]{1,0:T(8,128)(2,1)S(1)}, u32[]{:S(2)}, u32[]{:S(2)}) collective-permute-start(bf16[272,256]{1,0:T(8,128)(2,1)S(1)} %get-tuple-element.59), channel_id=1, source_target_pairs={{64,0},{17,1},{72,8},{49,33},{80,16},{81,65},{88,24},{113,97},{120... | collective-permute-start | bytes 417800 | tf_op jit(solution)/shard_map/ppermute | solution.py:573
  132.5 5.9 %collective-permute-done.13.t1 = bf16[272,128]{1,0:T(8,128)(2,1)S(1)} collective-permute-done((bf16[272,128]{1,0:T(8,128)(2,1)S(1)}, bf16[272,128]{1,0:T(8,128)(2,1)S(1)}, u32[]{:S(2)}, u32[]{:S(2)}) %collective-permute-start.13) | collective-permute-done | bytes 69664 | tf_op jit(solution)/shard_map/ppermute | solution.py:553
  143.1 3.3 %collective-permute-done.16.i1 = bf16[256,128]{1,0:T(8,128)(2,1)S(1)} collective-permute-done((bf16[256,128]{1,0:T(8,128)(2,1)S(1)}, bf16[256,128]{1,0:T(8,128)(2,1)S(1)}, u32[]{:S(2)}, u32[]{:S(2)}) %collective-permute-start.16) | collective-permute-done | bytes 65568 | tf_op jit(solution)/shard_map/ppermute | solution.py:555
  151.6 2.9 %shard_map.167 = (bf16[256,1024]{1,0:T(8,128)(2,1)}, f32[256,1024]{1,0:T(8,128)S(1)}, f32[256,1024]{1,0:T(8,128)S(1)}) custom-call(s32[12]{0:T(128)S(1)} %concatenate.13.index_ref, bf16[4,256,256]{2,1,0:T(8,128)(2,1)S(1)} %lin_final.1.lin, bf16[4,256,256]{2,1,0:T(8,128)(2,1)S(1)} %collective-permute-done.19.lin_other, ...), custom_call_target="tpu_custom_call" | custom-call | tf_op jit(solution)/shard_map/pallas_call | solution.py:472
  154.5 3.0 %collective-permute-start.40 = (bf16[256,1024]{1,0:T(8,128)(2,1)}, bf16[256,1024]{1,0:T(8,128)(2,1)S(1)}, u32[]{:S(2)}, u32[]{:S(2)}) collective-permute-start(bf16[256,1024]{1,0:T(8,128)(2,1)} %get-tuple-element.62), channel_id=1, source_target_pairs={{0,6},{1,3},{2,0},{3,5},{4,2},{5,7},{6,4},{7,1},{8,14},{9,11},{10,... | collective-permute-start | bytes 1572872 | tf_op jit(solution)/shard_map/ppermute | solution.py:585
  157.5 5.6 %collective-permute-done.41 = bf16[256,1024]{1,0:T(8,128)(2,1)S(1)} collective-permute-done((bf16[256,1024]{1,0:T(8,128)(2,1)S(1)}, bf16[256,1024]{1,0:T(8,128)(2,1)S(1)}, u32[]{:S(2)}, u32[]{:S(2)}) %collective-permute-start.41) | collective-permute-done | bytes 524320 | tf_op jit(solution)/shard_map/ppermute | solution.py:583
  166.6 7.0 %collective-permute-done.42 = bf16[256,1024]{1,0:T(8,128)(2,1)S(1)} collective-permute-done((bf16[256,1024]{1,0:T(8,128)(2,1)S(1)}, bf16[256,1024]{1,0:T(8,128)(2,1)S(1)}, u32[]{:S(2)}, u32[]{:S(2)}) %collective-permute-start.42) | collective-permute-done | bytes 524320 | tf_op jit(solution)/shard_map/ppermute | solution.py:586
  (143 shorter events, 49.6 us)
Async XLA Ops:
  0.7 15.1 %collective-permute-start.3 = (bf16[256,1024]{1,0:T(8,128)(2,1)}, bf16[256,1024]{1,0:T(8,128)(2,1)S(1)}, u32[]{:S(2)}, u32[]{:S(2)}) collective-permute-start(bf16[256,1024]{1,0:T(8,128)(2,1)} %bitcast.79), channel_id=1, source_target_pairs={{0,2},{2,4},{4,6},{6,0},{1,3},{3,5},{5,7},{7,1},{8,10},{10,12},{12... | collective-permute-start | bytes 1572872 | tf_op jit(solution)/shard_map/ppermute | solution.py:67
  2.4 13.8 %collective-permute-start.1 = (bf16[256,1024]{1,0:T(8,128)(2,1)}, bf16[256,1024]{1,0:T(8,128)(2,1)S(1)}, u32[]{:S(2)}, u32[]{:S(2)}) collective-permute-start(bf16[256,1024]{1,0:T(8,128)(2,1)} %bitcast.80), channel_id=1, source_target_pairs={{0,6},{2,0},{4,2},{6,4},{1,7},{3,1},{5,3},{7,5},{8,14},{10,8},{12,... | collective-permute-start | bytes 1572872 | tf_op jit(solution)/shard_map/ppermute | solution.py:67
  4.7 14.4 %collective-permute-start.8 = (bf16[16,256]{1,0:T(8,128)(2,1)S(1)}, bf16[16,256]{1,0:T(8,128)(2,1)S(1)}, u32[]{:S(2)}, u32[]{:S(2)}) collective-permute-start(bf16[16,256]{1,0:T(8,128)(2,1)S(1)} %get-tuple-element.91), channel_id=1, source_target_pairs={{0,4},{2,6},{4,0},{6,2},{1,5},{3,7},{5,1},{7,3},{8,12},{10,14},{12... | collective-permute-start | bytes 24584 | tf_op jit(solution)/shard_map/ppermute | solution.py:67
  6.6 13.2 %collective-permute-start.7 = (bf16[16,256]{1,0:T(8,128)(2,1)S(1)}, bf16[16,256]{1,0:T(8,128)(2,1)S(1)}, u32[]{:S(2)}, u32[]{:S(2)}) collective-permute-start(bf16[16,256]{1,0:T(8,128)(2,1)S(1)} %get-tuple-element.91), channel_id=1, source_target_pairs={{0,6},{2,0},{4,2},{6,4},{1,7},{3,1},{5,3},{7,5},{8,14},{10,8},{12,... | collective-permute-start | bytes 24584 | tf_op jit(solution)/shard_map/ppermute | solution.py:67
  7.7 20.1 %collective-permute-start = (bf16[256,1024]{1,0:T(8,128)(2,1)}, bf16[256,1024]{1,0:T(8,128)(2,1)}, u32[]{:S(2)}, u32[]{:S(2)}) collective-permute-start(bf16[256,1024]{1,0:T(8,128)(2,1)} %bitcast.81), channel_id=1, source_target_pairs={{0,1},{1,0},{2,3},{3,2},{4,5},{5,4},{6,7},{7,6},{8,9},{9,8},{10,11... | collective-permute-start | bytes 1572872 | tf_op jit(solution)/shard_map/ppermute | solution.py:71
  18.5 14.7 %collective-permute-start.6 = (bf16[256,1024]{1,0:T(8,128)(2,1)S(1)}, bf16[256,1024]{1,0:T(8,128)(2,1)}, u32[]{:S(2)}, u32[]{:S(2)}) collective-permute-start(bf16[256,1024]{1,0:T(8,128)(2,1)S(1)} %collective-permute-done.3.mine), channel_id=1, source_target_pairs={{0,1},{1,0},{2,3},{3,2},{4,5},{5,4},{6,7},{7,6},{8,9},{9,8},{10,11... | collective-permute-start | bytes 1572872 | tf_op jit(solution)/shard_map/ppermute | solution.py:71
  19.0 17.0 %collective-permute-start.2 = (bf16[256,1024]{1,0:T(8,128)(2,1)S(1)}, bf16[256,1024]{1,0:T(8,128)(2,1)}, u32[]{:S(2)}, u32[]{:S(2)}) collective-permute-start(bf16[256,1024]{1,0:T(8,128)(2,1)S(1)} %collective-permute-done.1.mine), channel_id=1, source_target_pairs={{0,1},{1,0},{2,3},{3,2},{4,5},{5,4},{6,7},{7,6},{8,9},{9,8},{10,11... | collective-permute-start | bytes 1572872 | tf_op jit(solution)/shard_map/ppermute | solution.py:71
  42.1 16.4 %collective-permute-start.27 = (bf16[256,512]{1,0:T(8,128)(2,1)S(1)}, bf16[256,512]{1,0:T(8,128)(2,1)S(1)}, u32[]{:S(2)}, u32[]{:S(2)}) collective-permute-start(bf16[256,512]{1,0:T(8,128)(2,1)S(1)} %get-tuple-element.72), channel_id=1, source_target_pairs={{0,64},{1,17},{8,72},{9,25},{16,80},{17,1},{24,88},{25,9},{32,96},... | collective-permute-start | bytes 786440 | tf_op jit(solution)/shard_map/ppermute | solution.py:537
  46.0 12.4 %collective-permute-start.28 = (bf16[256,512]{1,0:T(8,128)(2,1)S(1)}, bf16[256,512]{1,0:T(8,128)(2,1)S(1)}, u32[]{:S(2)}, u32[]{:S(2)}) collective-permute-start(bf16[256,512]{1,0:T(8,128)(2,1)S(1)} %get-tuple-element.73), channel_id=1, source_target_pairs={{0,96},{1,25},{8,104},{9,1},{16,112},{17,9},{24,120},{25,17},{32,0... | collective-permute-start | bytes 786440 | tf_op jit(solution)/shard_map/ppermute | solution.py:537
  46.7 11.5 %collective-permute-start.24 = (bf16[256,512]{1,0:T(8,128)(2,1)S(1)}, bf16[256,512]{1,0:T(8,128)(2,1)S(1)}, u32[]{:S(2)}, u32[]{:S(2)}) collective-permute-start(bf16[256,512]{1,0:T(8,128)(2,1)S(1)} %get-tuple-element.74), channel_id=1, source_target_pairs={{0,32},{1,9},{8,40},{9,17},{16,48},{17,25},{24,56},{25,1},{32,64},... | collective-permute-start | bytes 786440 | tf_op jit(solution)/shard_map/ppermute | solution.py:537
  58.3 28.9 %collective-permute-start.25 = (bf16[2,256,512]{2,1,0:T(8,128)(2,1)S(1)}, bf16[2,256,512]{2,1,0:T(8,128)(2,1)}, u32[]{:S(2)}, u32[]{:S(2)}) collective-permute-start(bf16[2,256,512]{2,1,0:T(8,128)(2,1)S(1)} %pad_maximum_fusion.4.refs_4_), channel_id=1, source_target_pairs={{0,8},{1,33},{8,16},{9,41},{16,24},{17,49},{24,0},{25,57},{32,40},... | collective-permute-start | bytes 1572872 | tf_op jit(solution)/shard_map/ppermute | solution.py:545
  58.5 28.9 %collective-permute-start.29 = (bf16[2,256,512]{2,1,0:T(8,128)(2,1)S(1)}, bf16[2,256,512]{2,1,0:T(8,128)(2,1)}, u32[]{:S(2)}, u32[]{:S(2)}) collective-permute-start(bf16[2,256,512]{2,1,0:T(8,128)(2,1)S(1)} %pad_maximum_fusion.5.refs_5_), channel_id=1, source_target_pairs={{0,24},{1,97},{8,0},{9,105},{16,8},{17,113},{24,16},{25,121},{32,5... | collective-permute-start | bytes 1572872 | tf_op jit(solution)/shard_map/ppermute | solution.py:548
  70.4 30.7 %collective-permute-start.32 = (bf16[2,256,512]{2,1,0:T(8,128)(2,1)S(1)}, bf16[2,256,512]{2,1,0:T(8,128)(2,1)}, u32[]{:S(2)}, u32[]{:S(2)}) collective-permute-start(bf16[2,256,512]{2,1,0:T(8,128)(2,1)S(1)} %pad_maximum_fusion.4.refs_4_), channel_id=1, source_target_pairs={{0,24},{1,97},{8,0},{9,105},{16,8},{17,113},{24,16},{25,121},{32,5... | collective-permute-start | bytes 1572872 | tf_op jit(solution)/shard_map/ppermute | solution.py:546
  73.4 30.5 %collective-permute-start.31 = (bf16[2,256,512]{2,1,0:T(8,128)(2,1)S(1)}, bf16[2,256,512]{2,1,0:T(8,128)(2,1)}, u32[]{:S(2)}, u32[]{:S(2)}) collective-permute-start(bf16[2,256,512]{2,1,0:T(8,128)(2,1)S(1)} %pad_maximum_fusion.5.refs_5_), channel_id=1, source_target_pairs={{0,8},{1,33},{8,16},{9,41},{16,24},{17,49},{24,0},{25,57},{32,40},... | collective-permute-start | bytes 1572872 | tf_op jit(solution)/shard_map/ppermute | solution.py:547
  73.4 13.8 %collective-permute-start.22 = (bf16[256,256]{1,0:T(8,128)(2,1)S(1)}, bf16[256,256]{1,0:T(8,128)(2,1)S(1)}, u32[]{:S(2)}, u32[]{:S(2)}) collective-permute-start(bf16[256,256]{1,0:T(8,128)(2,1)S(1)} %get-tuple-element.77), channel_id=1, source_target_pairs={{0,64},{1,17},{8,72},{33,49},{16,80},{65,81},{24,88},{97,113},{32,... | collective-permute-start | bytes 393224 | tf_op jit(solution)/shard_map/ppermute | solution.py:539
  87.3 28.1 %collective-permute-start.26 = (bf16[2,256,512]{2,1,0:T(8,128)(2,1)}, bf16[2,256,512]{2,1,0:T(8,128)(2,1)}, u32[]{:S(2)}, u32[]{:S(2)}) collective-permute-start(bf16[2,256,512]{2,1,0:T(8,128)(2,1)} %collective-permute-done.25.refs_6_), channel_id=1, source_target_pairs={{0,8},{1,33},{8,16},{9,41},{16,24},{17,49},{24,0},{25,57},{32,40},... | collective-permute-start | bytes 1572872 | tf_op jit(solution)/shard_map/ppermute | solution.py:549
  87.4 28.0 %collective-permute-start.30 = (bf16[2,256,512]{2,1,0:T(8,128)(2,1)}, bf16[2,256,512]{2,1,0:T(8,128)(2,1)}, u32[]{:S(2)}, u32[]{:S(2)}) collective-permute-start(bf16[2,256,512]{2,1,0:T(8,128)(2,1)} %collective-permute-done.29.refs_9_), channel_id=1, source_target_pairs={{0,24},{1,97},{8,0},{9,105},{16,8},{17,113},{24,16},{25,121},{32,5... | collective-permute-start | bytes 1572872 | tf_op jit(solution)/shard_map/ppermute | solution.py:550
  97.4 34.0 %collective-permute-start.15 = (bf16[272,128]{1,0:T(8,128)(2,1)S(1)}, bf16[272,128]{1,0:T(8,128)(2,1)S(1)}, u32[]{:S(2)}, u32[]{:S(2)}) collective-permute-start(bf16[272,128]{1,0:T(8,128)(2,1)S(1)} %get-tuple-element.38.t0), channel_id=1, source_target_pairs={{0,96},{32,0},{64,32},{96,64},{1,97},{33,1},{65,33},{97,65},{2,98}... | collective-permute-start | bytes 208904 | tf_op jit(solution)/shard_map/ppermute | solution.py:553
  101.1 31.4 %collective-permute-start.14 = (bf16[272,128]{1,0:T(8,128)(2,1)S(1)}, bf16[272,128]{1,0:T(8,128)(2,1)S(1)}, u32[]{:S(2)}, u32[]{:S(2)}) collective-permute-start(bf16[272,128]{1,0:T(8,128)(2,1)S(1)} %get-tuple-element.38.t0), channel_id=1, source_target_pairs={{0,64},{32,96},{64,0},{96,32},{1,65},{33,97},{65,1},{97,33},{2,66}... | collective-permute-start | bytes 208904 | tf_op jit(solution)/shard_map/ppermute | solution.py:553
  121.5 17.5 %collective-permute-start.33 = (bf16[272,256]{1,0:T(8,128)(2,1)S(1)}, bf16[272,256]{1,0:T(8,128)(2,1)S(1)}, u32[]{:S(2)}, u32[]{:S(2)}) collective-permute-start(bf16[272,256]{1,0:T(8,128)(2,1)S(1)} %get-tuple-element.57), channel_id=1, source_target_pairs={{0,0},{1,1},{8,8},{33,33},{16,16},{65,65},{24,24},{97,97},{56,32},... | collective-permute-start | bytes 417800 | tf_op jit(solution)/shard_map/ppermute | solution.py:573
  122.2 17.5 %collective-permute-start.34 = (bf16[272,256]{1,0:T(8,128)(2,1)S(1)}, bf16[272,256]{1,0:T(8,128)(2,1)S(1)}, u32[]{:S(2)}, u32[]{:S(2)}) collective-permute-start(bf16[272,256]{1,0:T(8,128)(2,1)S(1)} %get-tuple-element.58), channel_id=1, source_target_pairs={{32,0},{9,1},{40,8},{41,33},{48,16},{73,65},{56,24},{105,97},{88,3... | collective-permute-start | bytes 417800 | tf_op jit(solution)/shard_map/ppermute | solution.py:573
  122.8 16.8 %collective-permute-start.35 = (bf16[272,256]{1,0:T(8,128)(2,1)S(1)}, bf16[272,256]{1,0:T(8,128)(2,1)S(1)}, u32[]{:S(2)}, u32[]{:S(2)}) collective-permute-start(bf16[272,256]{1,0:T(8,128)(2,1)S(1)} %get-tuple-element.59), channel_id=1, source_target_pairs={{64,0},{17,1},{72,8},{49,33},{80,16},{81,65},{88,24},{113,97},{120... | collective-permute-start | bytes 417800 | tf_op jit(solution)/shard_map/ppermute | solution.py:573
  151.2 11.8 %collective-permute-start.41 = (bf16[256,1024]{1,0:T(8,128)(2,1)S(1)}, bf16[256,1024]{1,0:T(8,128)(2,1)S(1)}, u32[]{:S(2)}, u32[]{:S(2)}) collective-permute-start(bf16[256,1024]{1,0:T(8,128)(2,1)S(1)} %shard_map.168), channel_id=1, source_target_pairs={{0,2},{1,7},{2,4},{3,1},{4,6},{5,3},{6,0},{7,5},{8,10},{9,15},{10,... | collective-permute-start | bytes 1572872 | tf_op jit(solution)/shard_map/ppermute | solution.py:583
  154.5 12.1 %collective-permute-start.40 = (bf16[256,1024]{1,0:T(8,128)(2,1)}, bf16[256,1024]{1,0:T(8,128)(2,1)S(1)}, u32[]{:S(2)}, u32[]{:S(2)}) collective-permute-start(bf16[256,1024]{1,0:T(8,128)(2,1)} %get-tuple-element.62), channel_id=1, source_target_pairs={{0,6},{1,3},{2,0},{3,5},{4,2},{5,7},{6,4},{7,1},{8,14},{9,11},{10,... | collective-permute-start | bytes 1572872 | tf_op jit(solution)/shard_map/ppermute | solution.py:585
  (35 other events, 363.4 us)
where the time goes:
time: 175 us
  waiting for transfers between devices  59.4 us (34%)
  starting transfers between devices  57.7 us (33%)
  Pallas kernels  41.1 us (23%)
  local copies, waits for them, and re-layouts  10.3 us (6%)
  other arithmetic  5.01 us (3%)
    pallas_call x2, Pallas kernels, attend(): pl.pallas_call(partial(attend_kernel, near), in_specs=[scalars()] * 3 + [...  16.6 us
    ppermute x4, waiting for transfers between devices, shards(): lax.ppermute(piece(queries, r, k), GRID, query_perm(k))  14.9 us
    pallas_call x4, Pallas kernels, front(): pl.pallas_call(front_kernel, in_specs=[scalars()] + [whole()] * (len(oper...  11.4 us
    ppermute x4, starting transfers between devices, shards(): lax.ppermute(mix[k], GRID, query_perm(k, True))  9.82 us
    ppermute x5, waiting for transfers between devices, shift_fs(): return lax.ppermute(array, 'fs', ring(4, shift))  8.39 us
    ppermute x5, starting transfers between devices, shift_fs(): return lax.ppermute(array, 'fs', ring(4, shift))  7.64 us
    pallas_call x1, Pallas kernels, gla(): pl.pallas_call(gla_kernel, in_specs=[whole()] * 10, out_shape=(jax.ShapeD...  7.09 us
    ppermute x1, waiting for transfers between devices, shards(): lax.ppermute((last + passed.astype(f32)).astype(bf16), ROW, core_ring(1))  7.04 us
  transfers between devices with their start and end apart: 43, of which 12 were waited for; matrix products, arithmetic and copies ran while one was open for 6% of the time, Pallas kernels for 21%

commit v1 on v0

--- a/solution.py
+++ b/solution.py
@@ -1,4 +1,5 @@
 from functools import partial
+from types import SimpleNamespace
 
 import jax
 import jax.numpy as jnp
@@ -115,7 +116,6 @@
         front_kernel,
         in_specs=[scalars()] + [whole()] * (len(operands) - 1),
         out_shape=tuple(jax.ShapeDtypeStruct((ROWS, cols), bf16) for cols in (4 * KEY, 2 * KEY, 2048)),
-        name="front",
         compiler_params=params(14),
         cost_estimate=pl.CostEstimate(flops=1500000000, transcendentals=0, bytes_accessed=6000000),
     )(*operands)
@@ -193,7 +193,6 @@
             jax.ShapeDtypeStruct((4, VALUE + EXTRA, KEY), bf16),
         ),
         scratch_shapes=[pltpu.VMEM((4, ROWS, 2048), bf16), pltpu.VMEM((2048, 2 * KEY), bf16)],
-        name="gla",
         compiler_params=params(16),
         cost_estimate=pl.CostEstimate(flops=6000000000, transcendentals=0, bytes_accessed=9000000),
     )(*normed, shifts, *weights, bias)
@@ -229,7 +228,6 @@
         prefix_kernel,
         in_specs=[scalars()] + [whole()] * 4,
         out_shape=(jax.ShapeDtypeStruct((4,) + shape, f32), jax.ShapeDtypeStruct(shape, bf16)),
-        name="prefix",
         compiler_params=params(8),
     )(place, *parts)
 
@@ -252,7 +250,6 @@
         combine_kernel,
         in_specs=[scalars()] + [whole()] * 5,
         out_shape=tuple(jax.ShapeDtypeStruct((VALUE, KEY), bf16) for _ in range(4)),
-        name="combine",
         compiler_params=params(8),
     )(places, *totals, before)
 
@@ -273,7 +270,6 @@
         lin_kernel,
         in_specs=[scalars()] + [whole()] * 7,
         out_shape=jax.ShapeDtypeStruct((4, ROWS, VALUE), bf16),
-        name="lin_final",
         compiler_params=params(12),
     )(index, *states, local, carried, gain)
 
@@ -445,7 +441,6 @@
         in_specs=[scalars()] * 3 + [whole()] * 4 + [anywhere] * len(parts) + [whole()] * len(rest),
         out_shape=out_shape,
         scratch_shapes=scratch,
-        name="attend_near" if near else "attend_far",
         compiler_params=params(18),
         cost_estimate=pl.CostEstimate(flops=4000000000, transcendentals=0, bytes_accessed=4000000),
     )(ids, slot_ids, lam, *queries, *parts, *rest)
@@ -486,6 +481,29 @@
     z = lax.axis_index("sp_0")
     y = lax.axis_index("sp_1")
     head = x * 2 + c
+    k4 = jnp.arange(4, dtype=jnp.int32)
+    k16 = jnp.arange(16, dtype=jnp.int32)
+    r = jnp.where(c == 0, z, y)
+    q = jnp.where(c == 0, y, z)
+    p = (r - k4) & 3
+    source = jnp.where((p == 0) | (p == 3), q, 3 - q)
+    ids = jnp.where(c == 0, 4 * p + source, 4 * source + p)
+    away = jnp.where(k16 < 4, 0, jnp.where(k16 < 8, 1, jnp.where(k16 < 12, 3, 2)))
+    block_p = (r - k16) & 3
+    block_q = (q - away) & 3
+    slot_ids = jnp.where(c == 0, 4 * block_p + block_q, 4 * block_q + block_p)
+    pieces = jnp.stack([jnp.int32(2), 3 - 2 * c, 1 + 2 * c, jnp.int32(0)])
+    index = jnp.concatenate([pieces, (pieces + x - r) & 3, (pieces + x - q) & 3])
+    place = dict(
+        core=c.reshape(1), first=c == 0, ids=ids, near_ids=slot_ids[:12], far_ids=slot_ids[12:], index=index,
+        r_pieces=[(r + k - x) & 3 for k in range(4)], y_pieces=[(y + k - x) & 3 for k in range(4)],
+        y=y.reshape(1), zy=jnp.stack([z, y]), lin=(y - x - k4) & 3, order=(k4 - r) & 3,
+        own_columns=c * 1024, other_columns=(1 - c) * 1024,
+        head=head, bias_at=head * KEY,
+    )
+    positions = (z * 4 + y) * ROWS + jnp.arange(ROWS, dtype=jnp.int32)
+    tokens, place = lax.optimization_barrier((tokens, place))
+    place = SimpleNamespace(**place)
     own = tokens[0]
 
     from_low = shift_fs(own, 1)
@@ -493,31 +511,33 @@
     shifts = [jnp.pad(decay_shift.reshape(2, ROWS), ((0, EXTRA - 2), (0, 0)))]
     shifts += [shift_fs(shifts[0], 4 - d) for d in (1, 2, 3)]
 
-    positions = (z * 4 + y) * ROWS + jnp.arange(ROWS, dtype=jnp.int32)
     inv_freq = jnp.power(f32(rope_base), -jnp.arange(64, dtype=f32) * (2.0 / KEY))
     angles = positions.astype(f32)[:, None] * inv_freq[None, :]
     cos = jnp.cos(angles)
     sin = jnp.sin(angles)
     cos_t = jnp.concatenate([cos, cos], axis=1)
     sin_t = jnp.concatenate([-sin, sin], axis=1)
-    bias = lax.dynamic_slice_in_dim(decay_bias, head * KEY, KEY, 0).reshape(1, KEY)
-    lam = lax.dynamic_slice_in_dim(soft_lambda, head, 1, 0)
     gain = norm_gain.reshape(1, -1)
-    core = c.reshape(1)
+    core = place.core
+    bias = lax.dynamic_slice(decay_bias, (place.bias_at,), (KEY,), allow_negative_indices=False).reshape(1, KEY)
+    lam = lax.dynamic_slice(soft_lambda, (place.head,), (1,), allow_negative_indices=False)
 
     def run_front(chunk):
         other = swap(chunk)
         return front(core, chunk, other, gain, soft_key, soft_value, soft_query, cos_t, sin_t)
 
+    def columns_at(matrix, at, half):
+        return lax.dynamic_slice(matrix, (0, at), (matrix.shape[0], half), allow_negative_indices=False)
+
     def columns(matrix):
         half = matrix.shape[1] // 2
-        mine = lax.dynamic_slice_in_dim(matrix, c * half, half, 1)
-        return [mine, swap(lax.dynamic_slice_in_dim(matrix, (1 - c) * half, half, 1))]
+        mine = columns_at(matrix, place.own_columns, half)
+        return [mine, swap(columns_at(matrix, place.other_columns, half))]
 
     out_weight = jnp.concatenate(columns(lin_out) + columns(soft_out), axis=0)
 
     fronts = {0: run_front(own)}
-    passed = jnp.where(c == 0, from_low, from_high)
+    passed = jnp.where(place.first, from_low, from_high)
     from_far = lax.ppermute(passed, ROW, core_ring(1))
     fronts[1] = run_front(from_high)
     fronts[3] = run_front(from_low)
@@ -526,19 +546,18 @@
     kv, queries = jnp.stack(kv), jnp.stack(queries)
     local, carried, states = gla(normed, jnp.stack(shifts), (lin_value, lin_decay, lin_query, lin_key), bias)
 
-    r = jnp.where(c == 0, z, y)
-    q = jnp.where(c == 0, y, z)
-
-    def piece(stacked, place, k):
-        return lax.dynamic_index_in_dim(stacked, (place + k - x) & 3, 0, keepdims=False)
-
-    own_kv = [piece(kv, r, 0)]
+    def piece(stacked, at):
+        sizes = (1,) + stacked.shape[1:]
+        return lax.dynamic_slice(stacked, (at, 0, 0), sizes, allow_negative_indices=False)[0]
+
+    by_r, by_y = place.r_pieces, place.y_pieces
+    own_kv = [piece(kv, by_r[0])]
     for k in (1, 3, 2):
-        own_kv.append(lax.ppermute(piece(kv, r, k), GRID, axis_perm(k, True)))
+        own_kv.append(lax.ppermute(piece(kv, by_r[k]), GRID, axis_perm(k, True)))
     own_kv = [own_kv[n] for n in (0, 1, 3, 2)]
-    my_q = [lax.ppermute(piece(queries, r, k), GRID, query_perm(k)) for k in range(4)]
-    y_parts = [piece(states, y, 0)]
-    y_parts += [lax.ppermute(piece(states, y, k), "sp_1", ring(4, k)) for k in (1, 2, 3)]
+    my_q = [lax.ppermute(piece(queries, by_r[k]), GRID, query_perm(k)) for k in range(4)]
+    y_parts = [piece(states, by_y[0])]
+    y_parts += [lax.ppermute(piece(states, by_y[k]), "sp_1", ring(4, k)) for k in (1, 2, 3)]
 
     own_a = jnp.stack(own_kv[:2])
     own_b = jnp.stack(own_kv[2:])
@@ -549,35 +568,28 @@
     far_a = lax.ppermute(low_a, GRID, axis_perm(1, False))
     far_b = lax.ppermute(high_b, GRID, axis_perm(3, False))
 
-    before, total = prefix(y.reshape(1), y_parts)
+    before, total = prefix(place.y, y_parts)
     z_parts = [total] + [lax.ppermute(total, "sp_0", ring(4, k)) for k in (1, 2, 3)]
-    coming = combine(jnp.stack([z, y]), z_parts, before)
+    coming = combine(place.zy, z_parts, before)
     coming = [coming[0]] + [lax.ppermute(coming[k], "sp_1", ring(4, k)) for k in (1, 2, 3)]
-    k4 = jnp.arange(4, dtype=jnp.int32)
-    lin_mix = lin_final((y - x - k4) & 3, coming, local, carried, lin_gain.reshape(1, -1))
+    lin_mix = lin_final(place.lin, coming, local, carried, lin_gain.reshape(1, -1))
     lin_other = swap(lin_mix)
 
-    p = (r - k4) & 3
-    source = jnp.where((p == 0) | (p == 3), q, 3 - q)
-    ids = jnp.where(c == 0, 4 * p + source, 4 * source + p)
-    k16 = jnp.arange(16, dtype=jnp.int32)
-    away = jnp.where(k16 < 4, 0, jnp.where(k16 < 8, 1, jnp.where(k16 < 12, 3, 2)))
-    block_p = (r - k16) & 3
-    block_q = (q - away) & 3
-    slot_ids = jnp.where(c == 0, 4 * block_p + block_q, 4 * block_q + block_p)
     sums = attend(
-        True, ids, slot_ids[:12], lam, my_q, (own_a, own_b, low_a, low_b, high_a, high_b)
+        True, place.ids, place.near_ids, lam, my_q, (own_a, own_b, low_a, low_b, high_a, high_b)
     )
-    mix = attend(False, ids, slot_ids[12:], lam, my_q, (far_a, far_b), *sums, soft_gain.reshape(1, -1))
+    mix = attend(
+        False, place.ids, place.far_ids, lam, my_q, (far_a, far_b), *sums,
+        soft_gain.reshape(1, -1),
+    )
 
     soft_mix = jnp.stack([lax.ppermute(mix[k], GRID, query_perm(k, True)) for k in range(4)])
     lines = soft_mix[:, ROWS:].reshape(4, 2, 8, ROWS).astype(f32)
     mass_rows = lines[:, :, 0] + lines[:, :, 1] + lines[:, :, 2]
-    log_mass = mass_rows[(k4 - r) & 3].transpose(1, 0, 2)[None]
+    log_mass = mass_rows[place.order].transpose(1, 0, 2)[None]
 
     soft_other = swap(soft_mix)
-    pieces = jnp.stack([jnp.int32(2), 3 - 2 * c, 1 + 2 * c, jnp.int32(0)])
-    index = jnp.concatenate([pieces, (pieces + x - r) & 3, (pieces + x - q) & 3])
+    index = place.index
     rows = (lin_mix, lin_other, soft_mix, soft_other, out_weight)
     (far,) = out_call(send_kernel, (bf16,), index, *rows)
     passed = lax.ppermute(far, ROW, core_ring(1))

time: 175 us -> 164 us (0.937)
  waiting for transfers between devices: 59.4 us -> 54.2 us
  starting transfers between devices: 57.7 us -> 62.4 us
  local copies, waits for them, and re-layouts: 10.3 us -> 5.73 us
  Pallas kernels: 41.1 us -> 37.3 us
  other arithmetic: 5.01 us -> 2.69 us
    ppermute x3, starting transfers between devices: 6.56 us -> 16.1 us  [shards(): lax.ppermute(total, 'sp_0', ring(4, k))]
    ppermute x3, waiting for transfers between devices: 5.87 us -> 0.01 us  [shards(): lax.ppermute(total, 'sp_0', ring(4, k))]
    ppermute x10, waiting for transfers between devices: 19.9 us -> 14.4 us  [the longest x4 14.4 us: shards(): lax.ppermute(piece(queries, by_r[k]), GRID, query_perm(k))]
    ppermute x4, starting transfers between devices: 9.82 us -> 5.28 us  [shards(): lax.ppermute(mix[k], GRID, query_perm(k, True))]
    pallas_call x4, Pallas kernels: 11.4 us -> 8.34 us  [front(): pl.pallas_call(front_kernel, in_specs=[scalars()] + [whole()] * (len(oper...]
    ppermute x4, waiting for transfers between devices: 0.01 us -> 2.76 us  [shards(): lax.ppermute(mix[k], GRID, query_perm(k, True))]
    unnamed x33 -> x31, local copies, waits for them, and re-layouts: 4.03 us -> 1.9 us
    ppermute x3, starting transfers between devices: 3.31 us -> 1.41 us  [shards(): lax.ppermute(coming[k], 'sp_1', ring(4, k))]
  transfers between devices with their start and end apart: 43 -> 43, of which waited for: 12 -> 15; matrix products, arithmetic and copies ran while one was open for 6% -> 3% of each run, Pallas kernels for 21% -> 21%
where the time goes in v1:
time: 164 us
  starting transfers between devices  62.4 us (38%)
  waiting for transfers between devices  54.2 us (33%)
  Pallas kernels  37.3 us (23%)
  local copies, waits for them, and re-layouts  5.73 us (3%)
  other arithmetic  2.69 us (2%)
    pallas_call x2, Pallas kernels, attend(): pl.pallas_call(partial(attend_kernel, near), in_specs=[scalars()] * 3 + [...  16.5 us
    ppermute x3, starting transfers between devices, shards(): lax.ppermute(total, 'sp_0', ring(4, k))  16.1 us
    ppermute x4, waiting for transfers between devices, shards(): lax.ppermute(piece(queries, by_r[k]), GRID, query_perm(k))  14.4 us
    ppermute x1, waiting for transfers between devices, shards(): lax.ppermute((last + passed.astype(f32)).astype(bf16), ROW, core_ring(1))  8.86 us
    ppermute x5, waiting for transfers between devices, shift_fs(): return lax.ppermute(array, 'fs', ring(4, shift))  8.46 us
    pallas_call x4, Pallas kernels, front(): pl.pallas_call(front_kernel, in_specs=[scalars()] + [whole()] * (len(oper...  8.34 us
    ppermute x5, starting transfers between devices, shift_fs(): return lax.ppermute(array, 'fs', ring(4, shift))  7.57 us
    ppermute x1, waiting for transfers between devices, shards(): passed = lax.ppermute(far, ROW, core_ring(1))  7.18 us
  transfers between devices with their start and end apart: 43, of which 15 were waited for; matrix products, arithmetic and copies ran while one was open for 3% of the time, Pallas kernels for 21%

profile of v1, /device:TPU:0, one launch (start us, length us, event | category | flops | bytes accessed | tf_op | source)
XLA Modules:
  0.0 163.5 jit_solution(14447643638849043250)
XLA Ops:
  8.1 8.0 %collective-permute-done.3.mine = bf16[256,1024]{1,0:T(8,128)(2,1)S(1)} collective-permute-done((bf16[256,1024]{1,0:T(8,128)(2,1)}, bf16[256,1024]{1,0:T(8,128)(2,1)S(1)}, u32[]{:S(2)}, u32[]{:S(2)}) %collective-permute-start.3) | collective-permute-done | bytes 524320 | tf_op jit(solution)/shard_map/ppermute | solution.py:68
  20.7 6.3 %collective-permute-done.4.mine = bf16[256,1024]{1,0:T(8,128)(2,1)S(1)} collective-permute-done((bf16[256,1024]{1,0:T(8,128)(2,1)S(1)}, bf16[256,1024]{1,0:T(8,128)(2,1)S(1)}, u32[]{:S(2)}, u32[]{:S(2)}) %collective-permute-start.4) | collective-permute-done | bytes 524320 | tf_op jit(solution)/shard_map/ppermute | solution.py:541
  28.4 2.9 %shard_map.167 = (bf16[256,512]{1,0:T(8,128)(2,1)S(1)}, bf16[256,256]{1,0:T(8,128)(2,1)S(1)}, bf16[256,2048]{1,0:T(8,128)(2,1)S(1)}) custom-call(s32[1]{0:T(128)} %bitcast.core_ref, bf16[256,1024]{1,0:T(8,128)(2,1)S(1)} %bitcast.80, bf16[256,1024]{1,0:T(8,128)(2,1)} %collective-permute-done.other, f32[1,2048]{1,0:T(1,128)S(1)} %bitcast.81, ...), custom_call_target="tpu_custom_call" | custom-call | flops 1500000000 | bytes 6000000 | tf_op jit(solution)/shard_map/pallas_call | solution.py:115
  37.1 4.0 %collective-permute-start.27 = (bf16[256,512]{1,0:T(8,128)(2,1)S(1)}, bf16[256,512]{1,0:T(8,128)(2,1)S(1)}, u32[]{:S(2)}, u32[]{:S(2)}) collective-permute-start(bf16[256,512]{1,0:T(8,128)(2,1)S(1)} %get-tuple-element.118), channel_id=1, source_target_pairs={{0,64},{1,17},{8,72},{9,25},{16,80},{17,1},{24,88},{25,9},{32,96},... | collective-permute-start | bytes 786440 | tf_op jit(solution)/shard_map/ppermute | solution.py:556
  43.1 7.0 %shard_map.171 = (f32[4,256,256]{2,1,0:T(8,128)S(1)}, bf16[4,256,128]{2,1,0:T(8,128)(2,1)S(1)}, bf16[4,272,128]{2,1,0:T(8,128)(2,1)S(1)}) custom-call(bf16[256,2048]{1,0:T(8,128)(2,1)S(1)} %get-tuple-element.62.n0, bf16[256,2048]{1,0:T(8,128)(2,1)S(1)} %get-tuple-element.63.n1, bf16[256,2048]{1,0:T(8,128)(2,1)S(1)} %get-tuple-element.65.n2, ...), custom_call_target="tpu_custom_call" | custom-call | flops 6000000000 | bytes 9000000 | tf_op jit(solution)/shard_map/pallas_call | solution.py:187
  50.2 3.1 %collective-permute-start.12 = (bf16[272,128]{1,0:T(8,128)(2,1)S(1)}, bf16[272,128]{1,0:T(8,128)(2,1)S(1)}, u32[]{:S(2)}, u32[]{:S(2)}) collective-permute-start(bf16[272,128]{1,0:T(8,128)(2,1)S(1)} %get-tuple-element.126), channel_id=1, source_target_pairs={{0,24},{8,0},{16,8},{24,16},{1,25},{9,1},{17,9},{25,17},{2,26},{10... | collective-permute-start | bytes 208904 | tf_op jit(solution)/shard_map/ppermute | solution.py:560
  58.5 2.0 %collective-permute-start.23 = (bf16[256,256]{1,0:T(8,128)(2,1)S(1)}, bf16[256,256]{1,0:T(8,128)(2,1)S(1)}, u32[]{:S(2)}, u32[]{:S(2)}) collective-permute-start(bf16[256,256]{1,0:T(8,128)(2,1)S(1)} %get-tuple-element.122), channel_id=1, source_target_pairs={{0,96},{1,25},{8,104},{33,57},{16,112},{65,89},{24,120},{97,121},{... | collective-permute-start | bytes 393224 | tf_op jit(solution)/shard_map/ppermute | solution.py:558
  62.6 4.9 %collective-permute-done.23.refs_3_ = bf16[256,256]{1,0:T(8,128)(2,1)S(1)} collective-permute-done((bf16[256,256]{1,0:T(8,128)(2,1)S(1)}, bf16[256,256]{1,0:T(8,128)(2,1)S(1)}, u32[]{:S(2)}, u32[]{:S(2)}) %collective-permute-start.23) | collective-permute-done | bytes 131104 | tf_op jit(solution)/shard_map/ppermute | solution.py:558
  67.4 3.0 %collective-permute-start.22 = (bf16[256,256]{1,0:T(8,128)(2,1)S(1)}, bf16[256,256]{1,0:T(8,128)(2,1)S(1)}, u32[]{:S(2)}, u32[]{:S(2)}) collective-permute-start(bf16[256,256]{1,0:T(8,128)(2,1)S(1)} %get-tuple-element.123), channel_id=1, source_target_pairs={{0,64},{1,17},{8,72},{33,49},{16,80},{65,81},{24,88},{97,113},{32,... | collective-permute-start | bytes 393224 | tf_op jit(solution)/shard_map/ppermute | solution.py:558
  70.4 6.6 %collective-permute-done.22.refs_2_ = bf16[256,256]{1,0:T(8,128)(2,1)S(1)} collective-permute-done((bf16[256,256]{1,0:T(8,128)(2,1)S(1)}, bf16[256,256]{1,0:T(8,128)(2,1)S(1)}, u32[]{:S(2)}, u32[]{:S(2)}) %collective-permute-start.22) | collective-permute-done | bytes 131104 | tf_op jit(solution)/shard_map/ppermute | solution.py:558
  78.5 2.6 %collective-permute-start.30 = (bf16[2,256,512]{2,1,0:T(8,128)(2,1)S(1)}, bf16[2,256,512]{2,1,0:T(8,128)(2,1)S(1)}, u32[]{:S(2)}, u32[]{:S(2)}) collective-permute-start(bf16[2,256,512]{2,1,0:T(8,128)(2,1)S(1)} %collective-permute-done.29.refs_9_), channel_id=1, source_target_pairs={{0,24},{1,97},{8,0},{9,105},{16,8},{17,113},{24,16},{25,121},{32,5... | collective-permute-start | bytes 1572872 | tf_op jit(solution)/shard_map/ppermute | solution.py:569
  81.1 2.9 %collective-permute-done.21.refs_1_ = bf16[256,256]{1,0:T(8,128)(2,1)S(1)} collective-permute-done((bf16[256,256]{1,0:T(8,128)(2,1)S(1)}, bf16[256,256]{1,0:T(8,128)(2,1)S(1)}, u32[]{:S(2)}, u32[]{:S(2)}) %collective-permute-start.21) | collective-permute-done | bytes 131104 | tf_op jit(solution)/shard_map/ppermute | solution.py:558
  85.4 3.3 %collective-permute-start.15 = (bf16[272,128]{1,0:T(8,128)(2,1)S(1)}, bf16[272,128]{1,0:T(8,128)(2,1)S(1)}, u32[]{:S(2)}, u32[]{:S(2)}) collective-permute-start(bf16[272,128]{1,0:T(8,128)(2,1)S(1)} %get-tuple-element.73.t0), channel_id=1, source_target_pairs={{0,96},{32,0},{64,32},{96,64},{1,97},{33,1},{65,33},{97,65},{2,98}... | collective-permute-start | bytes 208904 | tf_op jit(solution)/shard_map/ppermute | solution.py:572
  88.7 6.9 %collective-permute-start.14 = (bf16[272,128]{1,0:T(8,128)(2,1)S(1)}, bf16[272,128]{1,0:T(8,128)(2,1)S(1)}, u32[]{:S(2)}, u32[]{:S(2)}) collective-permute-start(bf16[272,128]{1,0:T(8,128)(2,1)S(1)} %get-tuple-element.73.t0), channel_id=1, source_target_pairs={{0,64},{32,96},{64,0},{96,32},{1,65},{33,97},{65,1},{97,33},{2,66}... | collective-permute-start | bytes 208904 | tf_op jit(solution)/shard_map/ppermute | solution.py:572
  95.6 10.8 %shard_map.175 = (f32[4,2,256,256]{3,2,1,0:T(8,128)S(1)}, f32[4,2,8,256]{3,2,1,0:T(8,128)S(1)}, f32[4,2,8,256]{3,2,1,0:T(8,128)S(1)}) custom-call(s32[4]{0:T(128)S(1)} %get-tuple-element.81.ids_ref, s32[12]{0:T(128)S(1)} %bitcast.76, f32[1]{0:T(128)} %dynamic_slice.59.lam_ref, bf16[256,256]{1,0:T(8,128)(2,1)S(1)} %collective-permute-done.20.refs_0_, ...), custom_call_target="tpu_custom_call" | custom-call | flops 4000000000 | bytes 4000000 | tf_op jit(solution)/shard_map/pallas_call | solution.py:439
  106.5 5.7 %shard_map.176 = (bf16[272,256]{1,0:T(8,128)(2,1)S(1)}, bf16[272,256]{1,0:T(8,128)(2,1)S(1)}, bf16[272,256]{1,0:T(8,128)(2,1)S(1)}, bf16[272,256]{1,0:T(8,128)(2,1)S(1)}) custom-call(s32[4]{0:T(128)S(1)} %get-tuple-element.81.ids_ref, s32[4]{0:T(128)S(1)} %slice.18.slot_ids_ref, f32[1]{0:T(128)} %dynamic_slice.59.lam_ref, ...), custom_call_target="tpu_custom_call" | custom-call | flops 4000000000 | bytes 4000000 | tf_op jit(solution)/shard_map/pallas_call | solution.py:439
  113.8 5.9 %collective-permute-start.13 = (bf16[272,128]{1,0:T(8,128)(2,1)S(1)}, bf16[272,128]{1,0:T(8,128)(2,1)S(1)}, u32[]{:S(2)}, u32[]{:S(2)}) collective-permute-start(bf16[272,128]{1,0:T(8,128)(2,1)S(1)} %get-tuple-element.73.t0), channel_id=1, source_target_pairs={{0,32},{32,64},{64,96},{96,0},{1,33},{33,65},{65,97},{97,1},{2,34}... | collective-permute-start | bytes 208904 | tf_op jit(solution)/shard_map/ppermute | solution.py:572
  119.7 4.5 %collective-permute-start.35 = (bf16[272,256]{1,0:T(8,128)(2,1)S(1)}, bf16[272,256]{1,0:T(8,128)(2,1)S(1)}, u32[]{:S(2)}, u32[]{:S(2)}) collective-permute-start(bf16[272,256]{1,0:T(8,128)(2,1)S(1)} %get-tuple-element.102), channel_id=1, source_target_pairs={{64,0},{17,1},{72,8},{49,33},{80,16},{81,65},{88,24},{113,97},{120... | collective-permute-start | bytes 417800 | tf_op jit(solution)/shard_map/ppermute | solution.py:586
  128.1 2.3 %collective-permute-done.36 = bf16[272,256]{1,0:T(8,128)(2,1)S(1)} collective-permute-done((bf16[272,256]{1,0:T(8,128)(2,1)S(1)}, bf16[272,256]{1,0:T(8,128)(2,1)S(1)}, u32[]{:S(2)}, u32[]{:S(2)}) %collective-permute-start.36) | collective-permute-done | bytes 139296 | tf_op jit(solution)/shard_map/ppermute | solution.py:586
  130.6 2.5 %collective-permute-done.16.i1 = bf16[256,128]{1,0:T(8,128)(2,1)S(1)} collective-permute-done((bf16[256,128]{1,0:T(8,128)(2,1)S(1)}, bf16[256,128]{1,0:T(8,128)(2,1)S(1)}, u32[]{:S(2)}, u32[]{:S(2)}) %collective-permute-start.16) | collective-permute-done | bytes 65568 | tf_op jit(solution)/shard_map/ppermute | solution.py:574
  139.3 2.4 %shard_map.177 = (bf16[256,1024]{1,0:T(8,128)(2,1)S(1)}, f32[256,1024]{1,0:T(8,128)S(1)}, f32[256,1024]{1,0:T(8,128)S(1)}) custom-call(s32[12]{0:T(128)S(1)} %concatenate.13.index_ref, bf16[4,256,256]{2,1,0:T(8,128)(2,1)S(1)} %shard_map.174.lin, bf16[4,256,256]{2,1,0:T(8,128)(2,1)S(1)} %collective-permute-done.19.lin_other, ...), custom_call_target="tpu_custom_call" | custom-call | tf_op jit(solution)/shard_map/pallas_call | solution.py:467
  141.7 3.0 %collective-permute-start.40 = (bf16[256,1024]{1,0:T(8,128)(2,1)S(1)}, bf16[256,1024]{1,0:T(8,128)(2,1)S(1)}, u32[]{:S(2)}, u32[]{:S(2)}) collective-permute-start(bf16[256,1024]{1,0:T(8,128)(2,1)S(1)} %get-tuple-element.107), channel_id=1, source_target_pairs={{0,6},{1,3},{2,0},{3,5},{4,2},{5,7},{6,4},{7,1},{8,14},{9,11},{10,... | collective-permute-start | bytes 1572872 | tf_op jit(solution)/shard_map/ppermute | solution.py:597
  144.7 7.2 %collective-permute-done.41 = bf16[256,1024]{1,0:T(8,128)(2,1)S(1)} collective-permute-done((bf16[256,1024]{1,0:T(8,128)(2,1)S(1)}, bf16[256,1024]{1,0:T(8,128)(2,1)S(1)}, u32[]{:S(2)}, u32[]{:S(2)}) %collective-permute-start.41) | collective-permute-done | bytes 524320 | tf_op jit(solution)/shard_map/ppermute | solution.py:595
  153.6 8.9 %collective-permute-done.42 = bf16[256,1024]{1,0:T(8,128)(2,1)S(1)} collective-permute-done((bf16[256,1024]{1,0:T(8,128)(2,1)S(1)}, bf16[256,1024]{1,0:T(8,128)(2,1)S(1)}, u32[]{:S(2)}, u32[]{:S(2)}) %collective-permute-start.42) | collective-permute-done | bytes 524320 | tf_op jit(solution)/shard_map/ppermute | solution.py:598
  (140 shorter events, 45.7 us)
Async XLA Ops:
  1.1 15.0 %collective-permute-start.3 = (bf16[256,1024]{1,0:T(8,128)(2,1)}, bf16[256,1024]{1,0:T(8,128)(2,1)S(1)}, u32[]{:S(2)}, u32[]{:S(2)}) collective-permute-start(bf16[256,1024]{1,0:T(8,128)(2,1)} %bitcast.77), channel_id=1, source_target_pairs={{0,2},{2,4},{4,6},{6,0},{1,3},{3,5},{5,7},{7,1},{8,10},{10,12},{12... | collective-permute-start | bytes 1572872 | tf_op jit(solution)/shard_map/ppermute | solution.py:68
  2.7 13.8 %collective-permute-start.1 = (bf16[256,1024]{1,0:T(8,128)(2,1)}, bf16[256,1024]{1,0:T(8,128)(2,1)S(1)}, u32[]{:S(2)}, u32[]{:S(2)}) collective-permute-start(bf16[256,1024]{1,0:T(8,128)(2,1)} %bitcast.78), channel_id=1, source_target_pairs={{0,6},{2,0},{4,2},{6,4},{1,7},{3,1},{5,3},{7,5},{8,14},{10,8},{12,... | collective-permute-start | bytes 1572872 | tf_op jit(solution)/shard_map/ppermute | solution.py:68
  5.0 13.6 %collective-permute-start.8 = (bf16[16,256]{1,0:T(8,128)(2,1)S(1)}, bf16[16,256]{1,0:T(8,128)(2,1)S(1)}, u32[]{:S(2)}, u32[]{:S(2)}) collective-permute-start(bf16[16,256]{1,0:T(8,128)(2,1)S(1)} %get-tuple-element.137), channel_id=1, source_target_pairs={{0,4},{2,6},{4,0},{6,2},{1,5},{3,7},{5,1},{7,3},{8,12},{10,14},{12... | collective-permute-start | bytes 24584 | tf_op jit(solution)/shard_map/ppermute | solution.py:68
  6.9 12.4 %collective-permute-start.7 = (bf16[16,256]{1,0:T(8,128)(2,1)S(1)}, bf16[16,256]{1,0:T(8,128)(2,1)S(1)}, u32[]{:S(2)}, u32[]{:S(2)}) collective-permute-start(bf16[16,256]{1,0:T(8,128)(2,1)S(1)} %get-tuple-element.137), channel_id=1, source_target_pairs={{0,6},{2,0},{4,2},{6,4},{1,7},{3,1},{5,3},{7,5},{8,14},{10,8},{12,... | collective-permute-start | bytes 24584 | tf_op jit(solution)/shard_map/ppermute | solution.py:68
  8.1 19.1 %collective-permute-start = (bf16[256,1024]{1,0:T(8,128)(2,1)}, bf16[256,1024]{1,0:T(8,128)(2,1)}, u32[]{:S(2)}, u32[]{:S(2)}) collective-permute-start(bf16[256,1024]{1,0:T(8,128)(2,1)} %bitcast.79), channel_id=1, source_target_pairs={{0,1},{1,0},{2,3},{3,2},{4,5},{5,4},{6,7},{7,6},{8,9},{9,8},{10,11... | collective-permute-start | bytes 1572872 | tf_op jit(solution)/shard_map/ppermute | solution.py:72
  18.1 13.2 %collective-permute-start.6 = (bf16[256,1024]{1,0:T(8,128)(2,1)S(1)}, bf16[256,1024]{1,0:T(8,128)(2,1)S(1)}, u32[]{:S(2)}, u32[]{:S(2)}) collective-permute-start(bf16[256,1024]{1,0:T(8,128)(2,1)S(1)} %collective-permute-done.3.mine), channel_id=1, source_target_pairs={{0,1},{1,0},{2,3},{3,2},{4,5},{5,4},{6,7},{7,6},{8,9},{9,8},{10,11... | collective-permute-start | bytes 1572872 | tf_op jit(solution)/shard_map/ppermute | solution.py:72
  18.6 14.5 %collective-permute-start.2 = (bf16[256,1024]{1,0:T(8,128)(2,1)S(1)}, bf16[256,1024]{1,0:T(8,128)(2,1)S(1)}, u32[]{:S(2)}, u32[]{:S(2)}) collective-permute-start(bf16[256,1024]{1,0:T(8,128)(2,1)S(1)} %collective-permute-done.1.mine), channel_id=1, source_target_pairs={{0,1},{1,0},{2,3},{3,2},{4,5},{5,4},{6,7},{7,6},{8,9},{9,8},{10,11... | collective-permute-start | bytes 1572872 | tf_op jit(solution)/shard_map/ppermute | solution.py:72
  37.1 17.8 %collective-permute-start.27 = (bf16[256,512]{1,0:T(8,128)(2,1)S(1)}, bf16[256,512]{1,0:T(8,128)(2,1)S(1)}, u32[]{:S(2)}, u32[]{:S(2)}) collective-permute-start(bf16[256,512]{1,0:T(8,128)(2,1)S(1)} %get-tuple-element.118), channel_id=1, source_target_pairs={{0,64},{1,17},{8,72},{9,25},{16,80},{17,1},{24,88},{25,9},{32,96},... | collective-permute-start | bytes 786440 | tf_op jit(solution)/shard_map/ppermute | solution.py:556
  41.1 15.8 %collective-permute-start.28 = (bf16[256,512]{1,0:T(8,128)(2,1)S(1)}, bf16[256,512]{1,0:T(8,128)(2,1)S(1)}, u32[]{:S(2)}, u32[]{:S(2)}) collective-permute-start(bf16[256,512]{1,0:T(8,128)(2,1)S(1)} %get-tuple-element.119), channel_id=1, source_target_pairs={{0,96},{1,25},{8,104},{9,1},{16,112},{17,9},{24,120},{25,17},{32,0... | collective-permute-start | bytes 786440 | tf_op jit(solution)/shard_map/ppermute | solution.py:556
  41.8 12.1 %collective-permute-start.24 = (bf16[256,512]{1,0:T(8,128)(2,1)S(1)}, bf16[256,512]{1,0:T(8,128)(2,1)S(1)}, u32[]{:S(2)}, u32[]{:S(2)}) collective-permute-start(bf16[256,512]{1,0:T(8,128)(2,1)S(1)} %get-tuple-element.120), channel_id=1, source_target_pairs={{0,32},{1,9},{8,40},{9,17},{16,48},{17,25},{24,56},{25,1},{32,64},... | collective-permute-start | bytes 786440 | tf_op jit(solution)/shard_map/ppermute | solution.py:556
  55.0 22.1 %collective-permute-start.25 = (bf16[2,256,512]{2,1,0:T(8,128)(2,1)S(1)}, bf16[2,256,512]{2,1,0:T(8,128)(2,1)S(1)}, u32[]{:S(2)}, u32[]{:S(2)}) collective-permute-start(bf16[2,256,512]{2,1,0:T(8,128)(2,1)S(1)} %pad_maximum_fusion.4.refs_4_), channel_id=1, source_target_pairs={{0,8},{1,33},{8,16},{9,41},{16,24},{17,49},{24,0},{25,57},{32,40},... | collective-permute-start | bytes 1572872 | tf_op jit(solution)/shard_map/ppermute | solution.py:564
  57.0 21.5 %collective-permute-start.29 = (bf16[2,256,512]{2,1,0:T(8,128)(2,1)S(1)}, bf16[2,256,512]{2,1,0:T(8,128)(2,1)S(1)}, u32[]{:S(2)}, u32[]{:S(2)}) collective-permute-start(bf16[2,256,512]{2,1,0:T(8,128)(2,1)S(1)} %pad_maximum_fusion.5.refs_5_), channel_id=1, source_target_pairs={{0,24},{1,97},{8,0},{9,105},{16,8},{17,113},{24,16},{25,121},{32,5... | collective-permute-start | bytes 1572872 | tf_op jit(solution)/shard_map/ppermute | solution.py:567
  60.5 28.2 %collective-permute-start.32 = (bf16[2,256,512]{2,1,0:T(8,128)(2,1)S(1)}, bf16[2,256,512]{2,1,0:T(8,128)(2,1)S(1)}, u32[]{:S(2)}, u32[]{:S(2)}) collective-permute-start(bf16[2,256,512]{2,1,0:T(8,128)(2,1)S(1)} %pad_maximum_fusion.4.refs_4_), channel_id=1, source_target_pairs={{0,24},{1,97},{8,0},{9,105},{16,8},{17,113},{24,16},{25,121},{32,5... | collective-permute-start | bytes 1572872 | tf_op jit(solution)/shard_map/ppermute | solution.py:565
  62.3 33.3 %collective-permute-start.31 = (bf16[2,256,512]{2,1,0:T(8,128)(2,1)S(1)}, bf16[2,256,512]{2,1,0:T(8,128)(2,1)S(1)}, u32[]{:S(2)}, u32[]{:S(2)}) collective-permute-start(bf16[2,256,512]{2,1,0:T(8,128)(2,1)S(1)} %pad_maximum_fusion.5.refs_5_), channel_id=1, source_target_pairs={{0,8},{1,33},{8,16},{9,41},{16,24},{17,49},{24,0},{25,57},{32,40},... | collective-permute-start | bytes 1572872 | tf_op jit(solution)/shard_map/ppermute | solution.py:566
  77.0 29.4 %collective-permute-start.26 = (bf16[2,256,512]{2,1,0:T(8,128)(2,1)S(1)}, bf16[2,256,512]{2,1,0:T(8,128)(2,1)S(1)}, u32[]{:S(2)}, u32[]{:S(2)}) collective-permute-start(bf16[2,256,512]{2,1,0:T(8,128)(2,1)S(1)} %collective-permute-done.25.refs_6_), channel_id=1, source_target_pairs={{0,8},{1,33},{8,16},{9,41},{16,24},{17,49},{24,0},{25,57},{32,40},... | collective-permute-start | bytes 1572872 | tf_op jit(solution)/shard_map/ppermute | solution.py:568
  78.5 28.0 %collective-permute-start.30 = (bf16[2,256,512]{2,1,0:T(8,128)(2,1)S(1)}, bf16[2,256,512]{2,1,0:T(8,128)(2,1)S(1)}, u32[]{:S(2)}, u32[]{:S(2)}) collective-permute-start(bf16[2,256,512]{2,1,0:T(8,128)(2,1)S(1)} %collective-permute-done.29.refs_9_), channel_id=1, source_target_pairs={{0,24},{1,97},{8,0},{9,105},{16,8},{17,113},{24,16},{25,121},{32,5... | collective-permute-start | bytes 1572872 | tf_op jit(solution)/shard_map/ppermute | solution.py:569
  85.4 34.3 %collective-permute-start.15 = (bf16[272,128]{1,0:T(8,128)(2,1)S(1)}, bf16[272,128]{1,0:T(8,128)(2,1)S(1)}, u32[]{:S(2)}, u32[]{:S(2)}) collective-permute-start(bf16[272,128]{1,0:T(8,128)(2,1)S(1)} %get-tuple-element.73.t0), channel_id=1, source_target_pairs={{0,96},{32,0},{64,32},{96,64},{1,97},{33,1},{65,33},{97,65},{2,98}... | collective-permute-start | bytes 208904 | tf_op jit(solution)/shard_map/ppermute | solution.py:572
  88.7 35.5 %collective-permute-start.14 = (bf16[272,128]{1,0:T(8,128)(2,1)S(1)}, bf16[272,128]{1,0:T(8,128)(2,1)S(1)}, u32[]{:S(2)}, u32[]{:S(2)}) collective-permute-start(bf16[272,128]{1,0:T(8,128)(2,1)S(1)} %get-tuple-element.73.t0), channel_id=1, source_target_pairs={{0,64},{32,96},{64,0},{96,32},{1,65},{33,97},{65,1},{97,33},{2,66}... | collective-permute-start | bytes 208904 | tf_op jit(solution)/shard_map/ppermute | solution.py:572
  112.2 12.9 %collective-permute-start.33 = (bf16[272,256]{1,0:T(8,128)(2,1)S(1)}, bf16[272,256]{1,0:T(8,128)(2,1)S(1)}, u32[]{:S(2)}, u32[]{:S(2)}) collective-permute-start(bf16[272,256]{1,0:T(8,128)(2,1)S(1)} %get-tuple-element.100), channel_id=1, source_target_pairs={{0,0},{1,1},{8,8},{33,33},{16,16},{65,65},{24,24},{97,97},{56,32},... | collective-permute-start | bytes 417800 | tf_op jit(solution)/shard_map/ppermute | solution.py:586
  113.8 11.2 %collective-permute-start.13 = (bf16[272,128]{1,0:T(8,128)(2,1)S(1)}, bf16[272,128]{1,0:T(8,128)(2,1)S(1)}, u32[]{:S(2)}, u32[]{:S(2)}) collective-permute-start(bf16[272,128]{1,0:T(8,128)(2,1)S(1)} %get-tuple-element.73.t0), channel_id=1, source_target_pairs={{0,32},{32,64},{64,96},{96,0},{1,33},{33,65},{65,97},{97,1},{2,34}... | collective-permute-start | bytes 208904 | tf_op jit(solution)/shard_map/ppermute | solution.py:572
  125.0 10.8 %collective-permute-start.39 = (bf16[256,1024]{1,0:T(8,128)(2,1)S(1)}, bf16[256,1024]{1,0:T(8,128)(2,1)S(1)}, u32[]{:S(2)}, u32[]{:S(2)}) collective-permute-start(bf16[256,1024]{1,0:T(8,128)(2,1)S(1)} %get-tuple-element.117), channel_id=1, source_target_pairs={{0,1},{1,0},{2,3},{3,2},{4,5},{5,4},{6,7},{7,6},{8,9},{9,8},{10,11... | collective-permute-start | bytes 1572872 | tf_op jit(solution)/shard_map/ppermute | solution.py:72
  125.1 10.7 %collective-permute-start.38 = (bf16[256,1024]{1,0:T(8,128)(2,1)S(1)}, bf16[256,1024]{1,0:T(8,128)(2,1)S(1)}, u32[]{:S(2)}, u32[]{:S(2)}) collective-permute-start(bf16[256,1024]{1,0:T(8,128)(2,1)S(1)} %get-tuple-element.115), channel_id=1, source_target_pairs={{0,1},{1,0},{2,3},{3,2},{4,5},{5,4},{6,7},{7,6},{8,9},{9,8},{10,11... | collective-permute-start | bytes 1572872 | tf_op jit(solution)/shard_map/ppermute | solution.py:72
  139.0 12.9 %collective-permute-start.41 = (bf16[256,1024]{1,0:T(8,128)(2,1)S(1)}, bf16[256,1024]{1,0:T(8,128)(2,1)S(1)}, u32[]{:S(2)}, u32[]{:S(2)}) collective-permute-start(bf16[256,1024]{1,0:T(8,128)(2,1)S(1)} %shard_map.178), channel_id=1, source_target_pairs={{0,2},{1,7},{2,4},{3,1},{4,6},{5,3},{6,0},{7,5},{8,10},{9,15},{10,... | collective-permute-start | bytes 1572872 | tf_op jit(solution)/shard_map/ppermute | solution.py:595
  141.7 11.9 %collective-permute-start.40 = (bf16[256,1024]{1,0:T(8,128)(2,1)S(1)}, bf16[256,1024]{1,0:T(8,128)(2,1)S(1)}, u32[]{:S(2)}, u32[]{:S(2)}) collective-permute-start(bf16[256,1024]{1,0:T(8,128)(2,1)S(1)} %get-tuple-element.107), channel_id=1, source_target_pairs={{0,6},{1,3},{2,0},{3,5},{4,2},{5,7},{6,4},{7,1},{8,14},{9,11},{10,... | collective-permute-start | bytes 1572872 | tf_op jit(solution)/shard_map/ppermute | solution.py:597
  (34 other events, 366.6 us)
